TPU v7x, 128 devices: a whole 4x4x4 slice. The times are simulated.
128 devices in a mesh: sp: 16 (over z, y), dp: 8 (over x, core).
Axes of the slice: x: 4, y: 4, z: 4, core: 2. Of those that a mesh axis runs over, the one named last changes fastest.
Arguments:
- queries: bfloat16 [8, 2048, 3072], P('dp', 'sp'), may hold values from -20 to 20
- kv_latent: bfloat16 [8, 2048, 256], P('dp', 'sp'), may hold values from -60 to 60
- rope_key: bfloat16 [8, 2048, 32], P('dp', 'sp'), may hold values from -20 to 20
- latent_norm_gain: float32 [256], replicated, may hold values from 0.1 to 1.9
- key_up_weight: bfloat16 [256, 2048], replicated, may hold values from -0.375 to 0.375
- value_up_weight: bfloat16 [256, 2048], replicated, may hold values from -0.375 to 0.375
- out_proj: bfloat16 [2048, 2048], replicated, may hold values from -0.125 to 0.125
- residual: bfloat16 [8, 2048, 2048], P('dp', 'sp'), may hold values from -0.59765625 to 0.59765625
- ffn_gain: float32 [2048], replicated, may hold values from 0.1 to 1.9
- routes: int32 [8, 2048, 2], P('dp', 'sp'), may hold values from 0 to 127, all different within a row; in each aligned block of 128 rows (0 to 127, 128 to 255, ..., all dimensions but the last counted through in order) at most 4 rows name the same one
- route_weights: float32 [8, 2048, 2], P('dp', 'sp'), may hold values from 0.1 to 1
- expert_gate: bfloat16 [128, 2048, 1024], P(('sp', 'dp')), may hold values from -1.3258252 to 1.3258252
- expert_up: bfloat16 [128, 2048, 1024], P(('sp', 'dp')), may hold values from -1.3258252 to 1.3258252
- expert_down: bfloat16 [128, 1024, 2048], P(('sp', 'dp')), may hold values from -0.1875 to 0.1875
Outputs:
- normed_rows: bfloat16 [8, 2048, 2048], P('dp', 'sp')
- layer_out: bfloat16 [8, 2048, 2048], P('dp', 'sp')
Inputs may be any that keep to these rules, and one draw needn't show every extreme that they name: `routes`: each token names 2 different experts. Among the tokens of one device no expert is named more than 4 times, and in some devices' tokens an expert is named exactly 4 times.
All inputs are finite; a program needn't handle non-finite values.
Results may differ from a plain program's by a relative error of at most 0.012.
The roundings to bfloat16 on the way count: a program that leaves them out, or rounds other values in their place, can miss the bound.
Values may be sent and summed in bfloat16 or wider, within the bound.
No kernel may reach another device: no remote copies, remote signals or barrier semaphores. Data moves between devices by JAX's collectives and lax.ppermute only.
A program may use at most 128 MiB of HBM per device.

v0:
```python
import jax
import jax.numpy as jnp
from jax import lax
from jax.sharding import PartitionSpec as P

D = 2048
HEAD_COUNT = 32
PLAIN_HEAD_SIZE = 64
ROTARY_SIZE = 32
VALUE_HEAD_SIZE = 64
LATENT_WIDTH = 256
TOPK = 2
GRID_W = 64


eps_norm = 1e-06
rope_base = 10000.0
clamp_limit = 7.0
glu_alpha = 1.702


def in_order(blocks, dim):
    blocks = jnp.moveaxis(blocks, 0, dim)
    shape = blocks.shape
    return blocks.reshape(*shape[:dim], shape[dim] * shape[dim + 1], *shape[dim + 2 :])


def copy_for_each(array, axis):
    length = lax.axis_size(axis)
    return lax.all_to_all(
        jnp.broadcast_to(array[None], (length, *array.shape)), axis, 0, 0, tiled=True
    )


def gather_directly(array, axis, dim):
    return in_order(copy_for_each(array, axis), dim)


def rope_tables(positions):
    grid_row = (positions // GRID_W).astype(jnp.float32)
    grid_col = (positions % GRID_W).astype(jnp.float32)
    quarter = ROTARY_SIZE // 4
    frequency = rope_base ** (-(2.0 * jnp.arange(quarter, dtype=jnp.float32)) / (ROTARY_SIZE // 2))
    angles = jnp.concatenate(
        [grid_row[:, None] * frequency[None, :], grid_col[:, None] * frequency[None, :]], axis=1
    )
    return (jnp.cos(angles), jnp.sin(angles))


def rotate(entries, cosine_table, sine_table):
    pair_view = entries.reshape(entries.shape[:-1] + (entries.shape[-1] // 2, 2))
    first_half = pair_view[..., 0]
    second_half = pair_view[..., 1]
    turned = jnp.stack(
        [
            first_half * cosine_table - second_half * sine_table,
            first_half * sine_table + second_half * cosine_table,
        ],
        axis=-1,
    )
    return turned.reshape(entries.shape)


def rms_scale(entries, gain_vec):
    floats = entries.astype(jnp.float32)
    return (
        floats * lax.rsqrt(jnp.mean(floats * floats, axis=-1, keepdims=True) + eps_norm) * gain_vec
    )


def clamped_unit(gate_pre, up_pre):
    gate_cut = jnp.minimum(gate_pre, clamp_limit)
    up_cut = jnp.clip(up_pre, -clamp_limit, clamp_limit)
    return gate_cut * jax.nn.sigmoid(glu_alpha * gate_cut) * (up_cut + 1.0)


def expert_rows(rows, gate_w, up_w, down_w):
    gate_pre = jnp.dot(rows, gate_w, preferred_element_type=jnp.float32)
    up_pre = jnp.dot(rows, up_w, preferred_element_type=jnp.float32)
    hidden = clamped_unit(gate_pre, up_pre).astype(jnp.bfloat16)
    return jnp.dot(hidden, down_w, preferred_element_type=jnp.float32).astype(jnp.bfloat16)


def absorb_queries(q_rows, key_per_head):
    q_latent = jnp.einsum(
        "qhn,chn->qhc",
        q_rows[..., :PLAIN_HEAD_SIZE],
        key_per_head,
        preferred_element_type=jnp.float32,
    ).astype(jnp.bfloat16)
    return jnp.concatenate([q_latent, q_rows[..., PLAIN_HEAD_SIZE:]], axis=-1)


def attend_block(query_block, key_row_list, value_per_head):
    scores = jnp.einsum(
        "qhd,kd->hqk", query_block, key_row_list, preferred_element_type=jnp.float32
    )
    highest = jnp.max(scores, axis=-1, keepdims=True)
    weights = jnp.exp(scores - highest)
    weights_brain_float = (weights / jnp.sum(weights, axis=-1, keepdims=True)).astype(jnp.bfloat16)
    context = jnp.einsum(
        "nef,fg->eng",
        weights_brain_float,
        key_row_list[:, :LATENT_WIDTH],
        preferred_element_type=jnp.float32,
    ).astype(jnp.bfloat16)
    result = jnp.einsum(
        "qhc,chv->qhv", context, value_per_head, preferred_element_type=jnp.float32
    ).astype(jnp.bfloat16)
    return result.reshape(query_block.shape[0], query_block.shape[1] * VALUE_HEAD_SIZE)


def local(
    queries,
    kv_latent,
    rope_key,
    latent_norm_gain,
    key_up_weight,
    value_up_weight,
    out_proj,
    residual,
    ffn_gain,
    routes,
    route_weights,
    expert_gate,
    expert_up,
    expert_down,
):
    tok_rows = queries.shape[1]
    sp_size = lax.axis_size("sp")
    qk_width = PLAIN_HEAD_SIZE + ROTARY_SIZE
    score_scale = qk_width ** (-0.5)
    positions = lax.axis_index("sp") * tok_rows + jnp.arange(tok_rows, dtype=jnp.int32)
    cosine_table, sine_table = rope_tables(positions)
    query_float = queries[0].astype(jnp.float32).reshape(tok_rows, HEAD_COUNT, qk_width)
    query_turned = rotate(
        query_float[..., PLAIN_HEAD_SIZE:], cosine_table[:, None, :], sine_table[:, None, :]
    )
    q_ready = (
        jnp.concatenate([query_float[..., :PLAIN_HEAD_SIZE], query_turned], axis=-1) * score_scale
    ).astype(jnp.bfloat16)
    key_turned = rotate(rope_key[0].astype(jnp.float32), cosine_table, sine_table).astype(
        jnp.bfloat16
    )
    latent = rms_scale(kv_latent[0], latent_norm_gain).astype(jnp.bfloat16)
    packed = jnp.concatenate([latent, key_turned], axis=1)
    key_row_list = gather_directly(packed, "sp", 0)
    key_per_head = key_up_weight.reshape(LATENT_WIDTH, HEAD_COUNT, PLAIN_HEAD_SIZE)
    value_per_head = value_up_weight.reshape(LATENT_WIDTH, HEAD_COUNT, VALUE_HEAD_SIZE)
    group_size = 4
    group_count = HEAD_COUNT // group_size
    query_complete = absorb_queries(q_ready, key_per_head)
    q_groups = query_complete.reshape(
        tok_rows, group_count, group_size, LATENT_WIDTH + ROTARY_SIZE
    ).transpose(1, 0, 2, 3)
    value_groups = value_per_head.reshape(
        LATENT_WIDTH, group_count, group_size, VALUE_HEAD_SIZE
    ).transpose(1, 0, 2, 3)
    group_out = lax.map(
        lambda pair: attend_block(pair[0], key_row_list, pair[1]), (q_groups, value_groups)
    )
    tok_heads = group_out.transpose(1, 0, 2).reshape(tok_rows, HEAD_COUNT * VALUE_HEAD_SIZE)
    mixed = residual[0].astype(jnp.float32) + jnp.dot(
        tok_heads, out_proj, preferred_element_type=jnp.float32
    )
    normed = rms_scale(mixed, ffn_gain).astype(jnp.bfloat16)
    dp_size = lax.axis_size("dp")
    experts = sp_size * dp_size
    capacity = max(2, 2 * tok_rows * TOPK // experts)
    flat_expert = routes[0].reshape(-1)
    assigned = tok_rows * TOPK
    one_hot = (flat_expert[:, None] == jnp.arange(experts, dtype=jnp.int32)[None, :]).astype(
        jnp.int32
    )
    earlier = jnp.cumsum(one_hot, axis=0) - one_hot
    slot_rank = jnp.sum(earlier * one_hot, axis=1)
    slot_index = flat_expert * capacity + slot_rank
    slot_token = (
        jnp.full((experts * capacity,), tok_rows, jnp.int32)
        .at[slot_index]
        .set(jnp.arange(assigned, dtype=jnp.int32) // TOPK)
    )
    padded_rows = jnp.concatenate([normed, jnp.zeros((1, D), jnp.bfloat16)], axis=0)
    outgoing = padded_rows[slot_token].reshape(experts, capacity, D)
    gate_w = expert_gate[0]
    up_w = expert_up[0]
    down_w = expert_down[0]
    slot_rows = lax.all_to_all(outgoing, ("sp", "dp"), split_axis=0, concat_axis=0, tiled=True)
    item_shape = slot_rows.shape
    returned = lax.all_to_all(
        expert_rows(slot_rows.reshape(-1, D), gate_w, up_w, down_w).reshape(item_shape),
        ("sp", "dp"),
        split_axis=0,
        concat_axis=0,
        tiled=True,
    )
    expert_back = returned.reshape(experts * capacity, D)[slot_index].astype(jnp.float32)
    weighted = expert_back * route_weights[0].reshape(-1)[:, None]
    routed = jnp.sum(weighted.reshape(tok_rows, TOPK, D), axis=1)
    layer_out = (mixed + routed).astype(jnp.bfloat16)
    return (normed[None], layer_out[None])


def solution(mesh):
    in_specs = (
        P("dp", "sp", None),
        P("dp", "sp", None),
        P("dp", "sp", None),
        P(),
        P(),
        P(),
        P(),
        P("dp", "sp", None),
        P(),
        P("dp", "sp", None),
        P("dp", "sp", None),
        P(("sp", "dp"), None, None),
        P(("sp", "dp"), None, None),
        P(("sp", "dp"), None, None),
    )
    out_specs = (P("dp", "sp", None), P("dp", "sp", None))
    return jax.shard_map(local, mesh=mesh, in_specs=in_specs, out_specs=out_specs, check_vma=False)
```

profile of v0, /device:TPU:1, one launch (start us, length us, event | category | flops | bytes accessed | tf_op | source)
XLA Modules:
  0.0 228.1 jit_solution(4544953424549110556)
XLA Ops:
  3.9 1.2 broadcast_in_dim.16
  5.0 8.6 %all-to-all-start = ((bf16[16,128,288]{1,2,0:T(8,128)(2,1)}), bf16[16,128,288]{1,2,0:T(8,128)(2,1)}, u32[]{:S(2)}, u32[]{:S(2)}) async-start(bf16[16,128,288]{1,2,0:T(8,128)(2,1)} %broadcast_in_dim.16), calls=%async_computation | async-start | bytes 2359296 | tf_op jit(solution)/shard_map/all_to_all | solution.py:30
  14.1 1.5 copy.91
  16.9 2.1 convert_bitcast_fusion
  19.0 1.3 copy.92
  21.0 2.4 %pad_maximum_fusion = bf16[128,32,288]{2,0,1:T(8,128)(2,1)S(1)} fusion(bf16[128,32,32]{2,0,1:T(8,128)(2,1)} %copy.92, bf16[128,32,256]{2,0,1:T(8,128)(2,1)} %convert_bitcast_fusion), kind=kLoop, calls=%fused_computation.32 | loop fusion | flops 4718592 | bytes 4718592 | tf_op jit(solution)/shard_map/concatenate | solution.py:91
  23.6 2.7 %copy.93 = bf16[128,8,4,288]{0,3,2,1:T(8,128)(2,1)} copy(bf16[128,8,4,288]{3,0,2,1:T(8,128)(2,1)S(1)} %bitcast.135) | data formatting | bytes 4718592 | tf_op jit(solution)/shard_map/reshape | solution.py:153
  26.3 1.5 copy.89
  28.3 1.6 scatter_custom_fusion
  29.9 1.3 all-to-all-done
  31.2 1.8 copy.109
  33.0 74.7 %while.10 = (s32[]{:T(128)}, bf16[8,128,256]{1,2,0:T(8,128)(2,1)S(1)}, bf16[8,256,4,64]{1,3,2,0:T(8,128)(2,1)S(1)}, bf16[8,128,4,288]{1,3,2,0:T(8,128)(2,1)}, bf16[2048,288]{1,0:T(8,128)(2,1)S(1)}, /*index=5*/s32[]{:T(128)}) while((s32[]{:T(128)}, bf16[8,128,256]{1,2,0:T(8,128)(2,1)S(1)}, bf16[8,256,4,64]{1,3,2,0:T(8,128)(2,1)S(1)}, ...), condition=%wide.region_4.5_spmd, body=%wide.region_1.4_spmd.sunk | while | flops 1163039232 | bytes 36410468 | solution.py:159
  33.0 2.3 fusion.89
  36.1 1.1 copy-done
  37.2 5.1 %fusion.91 = bf16[4,64,128]{2,1,0:T(8,128)(2,1)S(1)} fusion(f32[4,128]{1,0:T(4,128)S(1)} %fusion.90, bf16[2048,288]{1,0:T(8,128)(2,1)S(1)} %get-tuple-element.120, bf16[8,256,4,64]{1,3,2,0:T(8,128)(2,1)S(1)} %get-tuple-element.118, s32[]{:T(128)} %get-tuple-element.110, f32[128,4,2048]{2,0,1:T(8,128)} %copy-done), kind=kOutput, calls=%fused_computation.15.clone.1 | convolution fusion | flops 556960256 | bytes 9636352 | tf_op jit(solution)/shard_map/while/body/eval_jaxpr/qhc,chv->qhv/dot_general | solution.py:107
  42.4 2.3 fusion.89
  45.5 1.1 copy-done
  46.6 5.1 %fusion.91 = bf16[4,64,128]{2,1,0:T(8,128)(2,1)S(1)} fusion(f32[4,128]{1,0:T(4,128)S(1)} %fusion.90, bf16[2048,288]{1,0:T(8,128)(2,1)S(1)} %get-tuple-element.120, bf16[8,256,4,64]{1,3,2,0:T(8,128)(2,1)S(1)} %get-tuple-element.118, s32[]{:T(128)} %get-tuple-element.110, f32[128,4,2048]{2,0,1:T(8,128)} %copy-done), kind=kOutput, calls=%fused_computation.15.clone.1 | convolution fusion | flops 556960256 | bytes 9636352 | tf_op jit(solution)/shard_map/while/body/eval_jaxpr/qhc,chv->qhv/dot_general | solution.py:107
  51.7 2.3 fusion.89
  54.8 1.1 copy-done
  55.9 5.1 %fusion.91 = bf16[4,64,128]{2,1,0:T(8,128)(2,1)S(1)} fusion(f32[4,128]{1,0:T(4,128)S(1)} %fusion.90, bf16[2048,288]{1,0:T(8,128)(2,1)S(1)} %get-tuple-element.120, bf16[8,256,4,64]{1,3,2,0:T(8,128)(2,1)S(1)} %get-tuple-element.118, s32[]{:T(128)} %get-tuple-element.110, f32[128,4,2048]{2,0,1:T(8,128)} %copy-done), kind=kOutput, calls=%fused_computation.15.clone.1 | convolution fusion | flops 556960256 | bytes 9636352 | tf_op jit(solution)/shard_map/while/body/eval_jaxpr/qhc,chv->qhv/dot_general | solution.py:107
  61.0 2.3 fusion.89
  64.2 1.1 copy-done
  65.3 5.1 %fusion.91 = bf16[4,64,128]{2,1,0:T(8,128)(2,1)S(1)} fusion(f32[4,128]{1,0:T(4,128)S(1)} %fusion.90, bf16[2048,288]{1,0:T(8,128)(2,1)S(1)} %get-tuple-element.120, bf16[8,256,4,64]{1,3,2,0:T(8,128)(2,1)S(1)} %get-tuple-element.118, s32[]{:T(128)} %get-tuple-element.110, f32[128,4,2048]{2,0,1:T(8,128)} %copy-done), kind=kOutput, calls=%fused_computation.15.clone.1 | convolution fusion | flops 556960256 | bytes 9636352 | tf_op jit(solution)/shard_map/while/body/eval_jaxpr/qhc,chv->qhv/dot_general | solution.py:107
  70.4 2.3 fusion.89
  74.6 5.1 %fusion.91 = bf16[4,64,128]{2,1,0:T(8,128)(2,1)S(1)} fusion(f32[4,128]{1,0:T(4,128)S(1)} %fusion.90, bf16[2048,288]{1,0:T(8,128)(2,1)S(1)} %get-tuple-element.120, bf16[8,256,4,64]{1,3,2,0:T(8,128)(2,1)S(1)} %get-tuple-element.118, s32[]{:T(128)} %get-tuple-element.110, f32[128,4,2048]{2,0,1:T(8,128)} %copy-done), kind=kOutput, calls=%fused_computation.15.clone.1 | convolution fusion | flops 556960256 | bytes 9636352 | tf_op jit(solution)/shard_map/while/body/eval_jaxpr/qhc,chv->qhv/dot_general | solution.py:107
  79.7 2.3 fusion.89
  82.8 1.1 copy-done
  83.9 5.1 %fusion.91 = bf16[4,64,128]{2,1,0:T(8,128)(2,1)S(1)} fusion(f32[4,128]{1,0:T(4,128)S(1)} %fusion.90, bf16[2048,288]{1,0:T(8,128)(2,1)S(1)} %get-tuple-element.120, bf16[8,256,4,64]{1,3,2,0:T(8,128)(2,1)S(1)} %get-tuple-element.118, s32[]{:T(128)} %get-tuple-element.110, f32[128,4,2048]{2,0,1:T(8,128)} %copy-done), kind=kOutput, calls=%fused_computation.15.clone.1 | convolution fusion | flops 556960256 | bytes 9636352 | tf_op jit(solution)/shard_map/while/body/eval_jaxpr/qhc,chv->qhv/dot_general | solution.py:107
  89.1 2.3 fusion.89
  92.2 1.1 copy-done
  93.3 5.1 %fusion.91 = bf16[4,64,128]{2,1,0:T(8,128)(2,1)S(1)} fusion(f32[4,128]{1,0:T(4,128)S(1)} %fusion.90, bf16[2048,288]{1,0:T(8,128)(2,1)S(1)} %get-tuple-element.120, bf16[8,256,4,64]{1,3,2,0:T(8,128)(2,1)S(1)} %get-tuple-element.118, s32[]{:T(128)} %get-tuple-element.110, f32[128,4,2048]{2,0,1:T(8,128)} %copy-done), kind=kOutput, calls=%fused_computation.15.clone.1 | convolution fusion | flops 556960256 | bytes 9636352 | tf_op jit(solution)/shard_map/while/body/eval_jaxpr/qhc,chv->qhv/dot_general | solution.py:107
  98.4 2.3 fusion.89
  102.6 5.1 %fusion.91 = bf16[4,64,128]{2,1,0:T(8,128)(2,1)S(1)} fusion(f32[4,128]{1,0:T(4,128)S(1)} %fusion.90, bf16[2048,288]{1,0:T(8,128)(2,1)S(1)} %get-tuple-element.120, bf16[8,256,4,64]{1,3,2,0:T(8,128)(2,1)S(1)} %get-tuple-element.118, s32[]{:T(128)} %get-tuple-element.110, f32[128,4,2048]{2,0,1:T(8,128)} %copy-done), kind=kOutput, calls=%fused_computation.15.clone.1 | convolution fusion | flops 556960256 | bytes 9636352 | tf_op jit(solution)/shard_map/while/body/eval_jaxpr/qhc,chv->qhv/dot_general | solution.py:107
  107.8 4.8 %multiply_reduce_fusion.1 = (f32[128]{0:T(128)S(1)}, f32[128,2048]{1,0:T(8,128)S(1)}) fusion(bf16[128,2048]{0,1:T(8,128)(2,1)S(1)} %bitcast.143, bf16[2048,2048]{1,0:T(8,128)(2,1)} %param.22, bf16[1,128,2048]{2,1,0:T(8,128)(2,1)} %param.23), kind=kOutput, calls=%fused_computation.42 | convolution fusion | flops 1074790272 | bytes 10486272 | tf_op jit(solution)/shard_map/dot_general | solution.py:163
  112.8 3.3 %gather_fusion = bf16[512,2048]{1,0:T(8,128)(2,1)} fusion(bf16[129,2048]{1,0:T(8,128)(2,1)S(1)} %concatenate.50, s32[1024]{0:T(1024)S(1)} %pad_clamp_fusion.1), kind=kCustom, calls=%fused_computation | custom fusion | bytes 4196352 | tf_op jit(solution)/shard_map/gather | solution.py:184
  116.1 2.7 %reshape.376 = bf16[128,4,2048]{2,1,0:T(4,128)(2,1)S(1)} reshape(bf16[512,2048]{1,0:T(8,128)(2,1)} %gather_fusion) | data formatting | bytes 4194304 | tf_op jit(solution)/shard_map/reshape | solution.py:184
  118.9 39.2 %all_to_all.15 = bf16[128,4,2048]{2,1,0:T(4,128)(2,1)} all-to-all(bf16[128,4,2048]{2,1,0:T(4,128)(2,1)S(1)} %reshape.376), channel_id=1, replica_groups=mesh['sp'=16,'dp'=8] {'sp','dp'}, dimensions={0} | all-to-all | bytes 4194304 | tf_op jit(solution)/shard_map/all_to_all | solution.py:188
  158.1 2.5 %reshape.377 = bf16[512,2048]{1,0:T(8,128)(2,1)S(1)} reshape(bf16[128,4,2048]{2,1,0:T(4,128)(2,1)} %all_to_all.15) | data formatting | bytes 4194304 | tf_op jit(solution)/shard_map/reshape | solution.py:191
  160.6 5.8 %fusion.32 = f32[512,1024]{1,0:T(8,128)} fusion(bf16[512,2048]{1,0:T(8,128)(2,1)S(1)} %reshape.377, bf16[1,2048,1024]{2,1,0:T(8,128)(2,1)} %param.28), kind=kOutput, calls=%fused_computation.28 | convolution fusion | flops 2147483648 | bytes 8388608 | tf_op jit(solution)/shard_map/dot_general | solution.py:79
  166.4 10.4 %fusion.36 = bf16[512,2048]{1,0:T(8,128)(2,1)} fusion(bf16[1,1024,2048]{2,1,0:T(8,128)(2,1)} %param.29, f32[512,1024]{1,0:T(8,128)} %fusion.32, bf16[512,2048]{1,0:T(8,128)(2,1)S(1)} %reshape.377, bf16[1,2048,1024]{2,1,0:T(8,128)(2,1)} %param.27), kind=kOutput, calls=%fused_computation.33 | convolution fusion | flops 4301258752 | bytes 14680064 | tf_op jit(solution)/shard_map/dot_general | solution.py:81
  176.8 4.1 %reshape.378 = bf16[128,4,2048]{2,1,0:T(4,128)(2,1)} reshape(bf16[512,2048]{1,0:T(8,128)(2,1)} %fusion.36) | data formatting | bytes 4194304 | tf_op jit(solution)/shard_map/reshape | solution.py:191
  180.9 5.6 %all-to-all-start.2 = ((bf16[128,4,2048]{2,1,0:T(4,128)(2,1)}), bf16[128,4,2048]{2,1,0:T(4,128)(2,1)}, u32[]{:S(2)}, u32[]{:S(2)}) async-start(bf16[128,4,2048]{2,1,0:T(4,128)(2,1)} %reshape.378), calls=%async_computation.2 | async-start | bytes 4194304 | tf_op jit(solution)/shard_map/all_to_all | solution.py:190
  187.6 29.2 %all-to-all-done.2 = bf16[128,4,2048]{2,1,0:T(4,128)(2,1)} async-done(((bf16[128,4,2048]{2,1,0:T(4,128)(2,1)}), bf16[128,4,2048]{2,1,0:T(4,128)(2,1)}, u32[]{:S(2)}, u32[]{:S(2)}) %all-to-all-start.2) | async-done | bytes 2097184 | tf_op jit(solution)/shard_map/all_to_all | solution.py:190
  216.8 2.5 %reshape.379 = bf16[512,2048]{1,0:T(8,128)(2,1)S(1)} reshape(bf16[128,4,2048]{2,1,0:T(4,128)(2,1)} %all-to-all-done.2) | data formatting | bytes 4194304 | tf_op jit(solution)/shard_map/reshape | solution.py:197
  219.3 2.3 %gather_fusion.1 = bf16[256,2048]{1,0:T(8,128)(2,1)} fusion(bf16[512,2048]{1,0:T(8,128)(2,1)S(1)} %reshape.379, s32[1024]{0:T(1024)S(1)} %pad_clamp_fusion), kind=kCustom, calls=%fused_computation.1 | custom fusion | bytes 2098176 | tf_op jit(solution)/shard_map/gather | solution.py:197
  221.7 2.4 %reshape.384 = f32[128,2,2048]{2,1,0:T(2,128)S(1)} reshape(bf16[256,2048]{1,0:T(8,128)(2,1)} %gather_fusion.1) | data formatting | bytes 3145728 | tf_op jit(solution)/shard_map/convert_element_type | solution.py:197
  224.0 3.2 %multiply_reduce_fusion = f32[128,2048]{1,0:T(8,128)S(1)} fusion(f32[128,2,2048]{2,1,0:T(2,128)S(1)} %reshape.384, f32[128,2]{1,0:T(8,128)S(1)} %copy.106), kind=kLoop, calls=%fused_computation.35 | loop fusion | flops 786432 | bytes 3146752 | tf_op jit(solution)/shard_map/reduce_sum | solution.py:199
  (84 shorter events, 17.2 us)
Async XLA Ops:
  1.7 11.9 %copy-start.2 = (bf16[1,128,3072]{2,1,0:T(8,128)(2,1)S(1)}, bf16[1,128,3072]{2,1,0:T(8,128)(2,1)}, u32[]{:S(2)}) copy-start(bf16[1,128,3072]{2,1,0:T(8,128)(2,1)} %param.16) | copy-start | bytes 2359300
  5.0 26.1 %all-to-all-start = ((bf16[16,128,288]{1,2,0:T(8,128)(2,1)}), bf16[16,128,288]{1,2,0:T(8,128)(2,1)}, u32[]{:S(2)}, u32[]{:S(2)}) async-start(bf16[16,128,288]{1,2,0:T(8,128)(2,1)} %broadcast_in_dim.16), calls=%async_computation | async-start | bytes 2359296 | tf_op jit(solution)/shard_map/all_to_all | solution.py:30
  16.9 3.5 %copy-start.4 = (s32[1,128,2]{1,2,0:T(2,128)S(1)}, s32[1,128,2]{1,2,0:T(2,128)}, u32[]{:S(2)}) copy-start(s32[1,128,2]{1,2,0:T(2,128)} %param.25) | copy-start | bytes 3076
  27.8 5.2 %copy-start.1 = (bf16[8,128,256]{1,2,0:T(8,128)(2,1)S(1)}, bf16[8,128,256]{1,2,0:T(8,128)(2,1)}, u32[]{:S(2)}) copy-start(bf16[8,128,256]{1,2,0:T(8,128)(2,1)} %custom-call.4) | copy-start | bytes 1572868
  35.3 1.9 copy-start
  44.7 1.9 copy-start
  54.0 1.9 copy-start
  63.3 1.9 copy-start
  72.7 1.9 copy-start
  82.0 1.9 copy-start
  91.3 1.9 copy-start
  100.7 1.9 copy-start
  107.7 4.8 %copy-start.3 = (f32[2048]{0:T(1024)S(1)}, f32[2048]{0:T(1024)}, u32[]{:S(2)}) copy-start(f32[2048]{0:T(1024)} %param.24) | copy-start | bytes 24580
  180.9 5.6 %copy-start.5 = (f32[1,128,2]{1,2,0:T(2,128)S(1)}, f32[1,128,2]{1,2,0:T(2,128)}, u32[]{:S(2)}) copy-start(f32[1,128,2]{1,2,0:T(2,128)} %param.26) | copy-start | bytes 3076
  180.9 35.8 %all-to-all-start.2 = ((bf16[128,4,2048]{2,1,0:T(4,128)(2,1)}), bf16[128,4,2048]{2,1,0:T(4,128)(2,1)}, u32[]{:S(2)}, u32[]{:S(2)}) async-start(bf16[128,4,2048]{2,1,0:T(4,128)(2,1)} %reshape.378), calls=%async_computation.2 | async-start | bytes 4194304 | tf_op jit(solution)/shard_map/all_to_all | solution.py:190
where the time goes:
time: 229 us; the launch traced here: 228 us
  matrix products  82 us (36%)
  local copies, waits for them, and re-layouts  43 us (19%)
  blocking collectives  39.2 us (17%)
  waiting for transfers between devices  30.4 us (13%)
  other arithmetic  18 us (8%)
  starting transfers between devices  14.2 us (6%)
    dot_general x8, matrix products, attend_block(): jnp.einsum('qhc,chv->qhv', context, value_per_head, preferred_element_typ...  40.7 us
    all_to_all x1, blocking collectives, local(): lax.all_to_all(outgoing, ('sp', 'dp'), split_axis=0, concat_axis=0, tiled...  39.2 us
    all_to_all x1, waiting for transfers between devices, local(): lax.all_to_all(expert_rows(slot_rows.reshape(-1, D), gate_w, up_w, down_w...  29.2 us
    dot_general x8, matrix products, attend_block(): jnp.einsum('qhd,kd->hqk', query_block, key_row_list, preferred_element_ty...  18.2 us
    dot_general x1, matrix products, expert_rows(): jnp.dot(hidden, down_w, preferred_element_type=jnp.float32)  10.4 us
    while x16, local copies, waits for them, and re-layouts  8.84 us
    all_to_all x1, starting transfers between devices, copy_for_each(): lax.all_to_all(jnp.broadcast_to(array[None], (length, *array.shape)), axi...  8.63 us
    sub x8, other arithmetic, attend_block(): weights = jnp.exp(scores - highest)  6.5 us
  transfers between devices with their start and end apart: 2, of which 2 were waited for; matrix products, arithmetic and copies ran while one was open for 7% of the time, Pallas kernels for 0%

commit v1 on v0

v1 whole, which is shorter than its diff:
```python
import numpy as np
import jax
import jax.numpy as jnp
from jax import lax
from jax.experimental import pallas as pl
from jax.experimental.pallas import tpu as pltpu
from jax.sharding import PartitionSpec as P

D = 2048
HEADS = 32
PLAIN = 64
ROT = 32
QK = PLAIN + ROT
LAT = 256
TOPK = 2
GRID_W = 64
FF = 1024
CAP = 4
GROUP = 4
EPS = 1e-06
CLAMP = 7.0
ALPHA = 1.702
LOG2E = 1.4426950408889634
BF = jnp.bfloat16
F32 = jnp.float32


def lane_tables(positions, lanes):
    lane = np.arange(lanes)
    if lanes == ROT:
        entry, plain = lane, np.zeros(lanes, bool)
    else:
        entry, plain = lane % QK - PLAIN, lane % QK < PLAIN
    pair = np.where(plain, 0, entry // 2)
    quarter = ROT // 4
    freq = (10000.0 ** (-(2.0 * (pair % quarter)) / (ROT // 2))).astype(np.float32)
    by_row = pair < quarter
    sign = np.where(plain, 0.0, np.where(entry % 2 == 0, -1.0, 1.0)).astype(np.float32)
    row = (positions // GRID_W).astype(F32)[:, None]
    col = (positions % GRID_W).astype(F32)[:, None]
    angle = jnp.where(by_row[None], row, col) * freq[None]
    cosine = jnp.where(plain[None], 1.0, jnp.cos(angle))
    return cosine, jnp.sin(angle) * sign[None]


def turn(x, cosine, sine):
    lanes = x.shape[-1]
    lane = lax.broadcasted_iota(jnp.int32, x.shape, 1)
    swapped = jnp.where(
        lane % 2 == 0, pltpu.roll(x, lanes - 1, 1), pltpu.roll(x, 1, 1)
    )
    return x * cosine + swapped * sine


def key_kernel(lat_ref, rope_ref, gain_ref, cos_ref, sin_ref, out_ref):
    lat = lat_ref[...].astype(F32)
    ms = jnp.mean(lat * lat, axis=-1, keepdims=True)
    latent = (lat * lax.rsqrt(ms + EPS) * gain_ref[...]).astype(BF)
    rope = rope_ref[...].astype(F32)
    wide = jnp.concatenate([rope] * 4, axis=1)
    cw = jnp.concatenate([cos_ref[...]] * 4, axis=1)
    sw = jnp.concatenate([sin_ref[...]] * 4, axis=1)
    turned = turn(wide, cw, sw)[:, :ROT].astype(BF)
    for i in range(out_ref.shape[0]):
        out_ref[i, :, :LAT] = latent
        out_ref[i, :, LAT:] = turned


def route_kernel(col_ref, row_ref, bcol_ref, brow_ref):
    n = col_ref.shape[0]
    sub = lax.broadcasted_iota(jnp.int32, (n, n), 0)
    lane = lax.broadcasted_iota(jnp.int32, (n, n), 1)
    e_c = [col_ref[:, k : k + 1] for k in range(2)]
    e_r = [row_ref[k : k + 1, :] for k in range(2)]
    same00 = e_c[0] == e_r[0]
    same11 = e_c[1] == e_r[1]
    one = lambda m: jnp.where(m, 1.0, 0.0)
    r0 = jnp.sum(one(same00 & (lane < sub)), axis=1, keepdims=True)
    r1 = jnp.sum(one(same11 & (lane < sub)), axis=1, keepdims=True) + jnp.sum(
        one(e_c[1] == e_r[0]), axis=1, keepdims=True
    )
    bcol_ref[:, 0:1] = e_c[0] * 8 + r0.astype(jnp.int32)
    bcol_ref[:, 1:2] = e_c[1] * 8 + r1.astype(jnp.int32)
    s0 = jnp.sum(one(same00 & (sub < lane)), axis=0, keepdims=True)
    s1 = jnp.sum(one(same11 & (sub < lane)), axis=0, keepdims=True) + jnp.sum(
        one(e_c[0] == e_r[1]), axis=0, keepdims=True
    )
    brow_ref[0:1, :] = e_r[0] * 8 + s0.astype(jnp.int32)
    brow_ref[1:2, :] = e_r[1] * 8 + s1.astype(jnp.int32)


def dot(a, b, dims):
    return lax.dot_general(a, b, (dims, ((), ())), preferred_element_type=F32)


def attend_kernel(
    q_ref, cos_ref, sin_ref, keys_ref, ku_ref, vu_ref, wo_ref, res_ref, gain_ref, brow_ref,
    mixed_ref, normed_ref, out_ref,
    klt_ref, qs_ref, acc_ref,
):
    g = pl.program_id(0)
    toks = q_ref.shape[0]

    @pl.when(g == 0)
    def _():
        klt_ref[...] = keys_ref[:, :LAT].T
        acc_ref[...] = res_ref[...].astype(F32)

    q = q_ref[...].astype(F32)
    qr = turn(q, cos_ref[...], sin_ref[...]) * (QK ** -0.5)
    q_ready = qr.astype(BF)
    q_rope = (qr * LOG2E).astype(BF)
    for j in range(GROUP):
        rows = slice(j * toks, (j + 1) * toks)
        qn = q_ready[:, j * QK : j * QK + PLAIN]
        ql = dot(qn, ku_ref[:, j * PLAIN : (j + 1) * PLAIN], ((1,), (1,)))
        qs_ref[rows, :LAT] = (ql * LOG2E).astype(BF)
        qs_ref[rows, LAT:] = q_rope[:, j * QK + PLAIN : (j + 1) * QK]
    outs = []
    width = 2 * toks
    for half in range(GROUP // 2):
        cols = slice(half * width, (half + 1) * width)
        scores = dot(keys_ref[...], qs_ref[cols, :], ((1,), (1,)))
        top = jnp.max(scores, axis=0, keepdims=True)
        probs = jnp.exp2(scores - top)
        total = jnp.sum(probs, axis=0, keepdims=True)
        ctx = dot(klt_ref[...], probs.astype(BF), ((1,), (0,)))
        ctx = (ctx * (1.0 / total)).astype(BF)
        for j in range(2):
            h = half * 2 + j
            outs.append(
                dot(
                    vu_ref[:, h * PLAIN : (h + 1) * PLAIN],
                    ctx[:, j * toks : (j + 1) * toks],
                    ((0,), (0,)),
                ).astype(BF)
            )
    heads = jnp.concatenate(outs, axis=0)
    acc_ref[...] += dot(heads, wo_ref[...], ((0,), (0,)))

    @pl.when(g == pl.num_programs(0) - 1)
    def _():
        mixed = acc_ref[...]
        mixed_ref[...] = mixed
        ms = jnp.mean(mixed * mixed, axis=-1, keepdims=True)
        normed = (mixed * lax.rsqrt(ms + EPS) * gain_ref[...]).astype(BF)
        normed_ref[...] = normed
        n_rows = out_ref.shape[0]
        half_d = D // 2
        stacked = jnp.concatenate([normed[:, :half_d], normed[:, half_d:]], axis=0)
        row = lax.broadcasted_iota(jnp.int32, (n_rows, toks), 0)
        picks = []
        for h in range(2):
            m = (row == brow_ref[0:1, :] + 4 * h) | (row == brow_ref[1:2, :] + 4 * h)
            picks.append(jnp.where(m, 1.0, 0.0).astype(BF))
        pick = jnp.concatenate(picks, axis=1)
        out_ref[...] = dot(pick, stacked, ((1,), (0,))).astype(BF)


def expert_kernel(rows_ref, gate_ref, up_ref, down_ref, out_ref, x_ref, acc_ref):
    f = pl.program_id(0)
    n_src = rows_ref.shape[0]
    half_d = D // 2

    @pl.when(f == 0)
    def _():
        r = rows_ref[...].astype(F32).reshape(n_src // 2, 2, 8, half_d)
        a = r[:, 0].reshape(n_src * 4, half_d)
        b = r[:, 1].reshape(n_src * 4, half_d)
        sub = lax.broadcasted_iota(jnp.int32, a.shape, 0) % 8
        rolled = lambda v: pltpu.roll(v.reshape(n_src // 2, 8, half_d), 4, 1).reshape(v.shape)
        x_ref[:, :half_d] = jnp.where(sub < 4, a, rolled(b)).astype(BF)
        x_ref[:, half_d:] = jnp.where(sub < 4, rolled(a), b).astype(BF)

    x = x_ref[...]
    gate = dot(x, gate_ref[...], ((1,), (0,)))
    up = dot(x, up_ref[...], ((1,), (0,)))
    cut = jnp.minimum(gate, CLAMP)
    hidden = (cut * jax.nn.sigmoid(ALPHA * cut) * (jnp.clip(up, -CLAMP, CLAMP) + 1.0)).astype(BF)
    part = dot(hidden, down_ref[...], ((1,), (0,)))

    @pl.when(f == 0)
    def _():
        acc_ref[...] = part

    @pl.when(f > 0)
    def _():
        acc_ref[...] += part

    @pl.when(f == pl.num_programs(0) - 1)
    def _():
        lo = acc_ref[:, :half_d].reshape(n_src // 2, 8, half_d)
        hi = acc_ref[:, half_d:].reshape(n_src // 2, 8, half_d)
        sub = lax.broadcasted_iota(jnp.int32, lo.shape, 1)
        first = jnp.where(sub < 4, lo, pltpu.roll(hi, 4, 1))
        second = jnp.where(sub < 4, pltpu.roll(lo, 4, 1), hi)
        both = jnp.concatenate([first[:, None], second[:, None]], axis=1)
        out_ref[...] = both.reshape(n_src, 8, half_d).astype(BF)


def combine_kernel(rows_ref, bcol_ref, weight_ref, mixed_ref, out_ref):
    n_rows = rows_ref.shape[0]
    toks = mixed_ref.shape[0]
    half_d = D // 2
    lane = lax.broadcasted_iota(jnp.int32, (toks, n_rows), 1)
    for h in range(2):
        total = mixed_ref[:, h * half_d : (h + 1) * half_d]
        for k in range(TOPK):
            pick = jnp.where(lane == bcol_ref[:, k : k + 1] + 4 * h, 1.0, 0.0).astype(BF)
            total += weight_ref[:, k : k + 1] * dot(pick, rows_ref[...], ((1,), (0,)))
        out_ref[:, h * half_d : (h + 1) * half_d] = total.astype(BF)


def full(*shape):
    return pl.BlockSpec(shape, lambda *_: (0,) * len(shape))


def params(mb=60):
    return pltpu.CompilerParams(vmem_limit_bytes=mb * 1024 * 1024)


def local(
    queries, kv_latent, rope_key, latent_norm_gain, key_up_weight, value_up_weight, out_proj,
    residual, ffn_gain, routes, route_weights, expert_gate, expert_up, expert_down,
):
    toks = queries.shape[1]
    sp = lax.axis_size("sp")
    experts = sp * lax.axis_size("dp")
    keys_n = sp * toks
    sds = jax.ShapeDtypeStruct
    positions = lax.axis_index("sp") * toks + jnp.arange(toks, dtype=jnp.int32)
    kc, ks = lane_tables(positions, ROT)
    packed = pl.pallas_call(
        key_kernel, out_shape=sds((sp, toks, LAT + ROT), BF), compiler_params=params(), name="keys"
    )(kv_latent[0], rope_key[0], latent_norm_gain[None], kc, ks)
    keys = lax.all_to_all(packed, "sp", 0, 0, tiled=True).reshape(keys_n, LAT + ROT)

    qc, qs = lane_tables(positions, GROUP * QK)
    bcol, brow = pl.pallas_call(
        route_kernel,
        out_shape=(sds((toks, TOPK), jnp.int32), sds((TOPK, toks), jnp.int32)),
        compiler_params=params(),
        name="routes",
    )(routes[0], routes[0].T)

    steps = HEADS // GROUP
    mixed, normed, outgoing = pl.pallas_call(
        attend_kernel,
        grid=(steps,),
        in_specs=[
            pl.BlockSpec((toks, GROUP * QK), lambda g: (0, g)),
            full(toks, GROUP * QK),
            full(toks, GROUP * QK),
            full(keys_n, LAT + ROT),
            pl.BlockSpec((LAT, GROUP * PLAIN), lambda g: (0, g)),
            pl.BlockSpec((LAT, GROUP * PLAIN), lambda g: (0, g)),
            pl.BlockSpec((GROUP * PLAIN, D), lambda g: (g, 0)),
            full(toks, D),
            full(1, D),
            full(TOPK, toks),
        ],
        out_specs=(full(toks, D), full(toks, D), full(experts * 8, D // 2)),
        out_shape=(sds((toks, D), F32), sds((toks, D), BF), sds((experts * 8, D // 2), BF)),
        scratch_shapes=[
            pltpu.VMEM((LAT, keys_n), BF),
            pltpu.VMEM((GROUP * toks, LAT + ROT), BF),
            pltpu.VMEM((toks, D), F32),
        ],
        compiler_params=params(),
        name="attend",
    )(queries[0], qc, qs, keys, key_up_weight, value_up_weight, out_proj, residual[0],
      ffn_gain[None], brow)

    slot_rows = lax.all_to_all(
        outgoing.reshape(experts, 8, D // 2), ("sp", "dp"), 0, 0, tiled=True
    )
    f_steps = 4
    fb = FF // f_steps
    expert_out = pl.pallas_call(
        expert_kernel,
        grid=(f_steps,),
        in_specs=[
            full(experts, 8, D // 2),
            pl.BlockSpec((D, fb), lambda f: (0, f)),
            pl.BlockSpec((D, fb), lambda f: (0, f)),
            pl.BlockSpec((fb, D), lambda f: (f, 0)),
        ],
        out_specs=full(experts, 8, D // 2),
        out_shape=sds((experts, 8, D // 2), BF),
        scratch_shapes=[pltpu.VMEM((experts * CAP, D), BF), pltpu.VMEM((experts * CAP, D), F32)],
        compiler_params=params(),
        name="experts",
    )(slot_rows, expert_gate[0], expert_up[0], expert_down[0])
    returned = lax.all_to_all(expert_out, ("sp", "dp"), 0, 0, tiled=True)
    layer_out = pl.pallas_call(
        combine_kernel,
        out_shape=sds((toks, D), BF),
        compiler_params=params(),
        name="combine",
    )(returned.reshape(experts * 8, D // 2), bcol, route_weights[0], mixed)
    return normed[None], layer_out[None]


def solution(mesh):
    tok = P("dp", "sp", None)
    exp = P(("sp", "dp"), None, None)
    in_specs = (
        tok, tok, tok, P(), P(), P(), P(), tok, P(), tok, tok, exp, exp, exp,
    )
    return jax.shard_map(
        local, mesh=mesh, in_specs=in_specs, out_specs=(tok, tok), check_vma=False
    )
```

time: 229 us -> 176 us (0.77)
  matrix products: 82 us -> 0 us
  Pallas kernels: 0 us -> 68.1 us
  local copies, waits for them, and re-layouts: 43 us -> 8.31 us
  other arithmetic: 18 us -> 3.2 us
  waiting for transfers between devices: 30.4 us -> 43.3 us
    dot_general x20 -> x0, matrix products: 82 us -> none  [the longest x8 40.7 us: attend_block(): jnp.einsum('qhc,chv->qhv', context, value_per_head, preferred_element_typ...]
    pallas_call x0 -> x5, Pallas kernels: none -> 68.1 us  [the longest x1 45.8 us: local(): pl.pallas_call(attend_kernel, grid=(steps,), in_specs=[pl.BlockSpec((toks...]
    reshape x5 -> x0, local copies, waits for them, and re-layouts: 14.7 us -> none  [the longest x1 4.12 us: local(): expert_rows(slot_rows.reshape(-1, D), gate_w, up_w, down_w)]
    all_to_all x2, waiting for transfers between devices: 30.4 us -> 43.3 us  [the longest x1 29.9 us: local(): returned = lax.all_to_all(expert_out, ('sp', 'dp'), 0, 0, tiled=True)]
    while x17 -> x0, local copies, waits for them, and re-layouts: 10.6 us -> none
    sub x9 -> x0, other arithmetic: 7.05 us -> none  [the longest x8 6.5 us: attend_block(): weights = jnp.exp(scores - highest)]
    gather x2 -> x0, local copies, waits for them, and re-layouts: 5.7 us -> none  [the longest x1 3.35 us: local(): outgoing = padded_rows[slot_token].reshape(experts, capacity, D)]
    reduce_sum x3 -> x0, other arithmetic: 4.36 us -> none  [the longest x1 3.16 us: local(): routed = jnp.sum(weighted.reshape(tok_rows, TOPK, D), axis=1)]
  transfers between devices with their start and end apart: 2 -> 2, of which waited for: 2 -> 2; matrix products, arithmetic and copies ran while one was open for 7% -> 2% of each run, Pallas kernels for 0% -> 1%
where the time goes in v1:
time: 176 us; the launch traced here: 175 us
  Pallas kernels  68.1 us (39%)
  waiting for transfers between devices  43.3 us (25%)
  blocking collectives  38.3 us (22%)
  starting transfers between devices  13.1 us (7%)
  local copies, waits for them, and re-layouts  8.31 us (5%)
  other arithmetic  3.2 us (2%)
    pallas_call x1, Pallas kernels, local(): pl.pallas_call(attend_kernel, grid=(steps,), in_specs=[pl.BlockSpec((toks...  45.8 us
    all_to_all x1, blocking collectives, local(): lax.all_to_all(outgoing.reshape(experts, 8, D // 2), ('sp', 'dp'), 0, 0,...  38.3 us
    all_to_all x1, waiting for transfers between devices, local(): returned = lax.all_to_all(expert_out, ('sp', 'dp'), 0, 0, tiled=True)  29.9 us
    pallas_call x1, Pallas kernels, local(): pl.pallas_call(expert_kernel, grid=(f_steps,), in_specs=[full(experts, 8,...  14.1 us
    all_to_all x1, waiting for transfers between devices, local(): lax.all_to_all(packed, 'sp', 0, 0, tiled=True).reshape(keys_n, LAT + ROT)  13.5 us
    all_to_all x1, starting transfers between devices, local(): lax.all_to_all(packed, 'sp', 0, 0, tiled=True).reshape(keys_n, LAT + ROT)  8.59 us
    all_to_all x1, starting transfers between devices, local(): returned = lax.all_to_all(expert_out, ('sp', 'dp'), 0, 0, tiled=True)  4.54 us
    pallas_call x1, Pallas kernels, local(): pl.pallas_call(combine_kernel, out_shape=sds((toks, D), BF), compiler_par...  4.05 us
  transfers between devices with their start and end apart: 2, of which 2 were waited for; matrix products, arithmetic and copies ran while one was open for 2% of the time, Pallas kernels for 1%

profile of v1, /device:TPU:1, one launch (start us, length us, event | category | flops | bytes accessed | tf_op | source)
XLA Modules:
  0.0 175.0 jit_solution(2247135189264598203)
XLA Ops:
  0.7 1.4 copy.32
  2.1 1.7 sine_multiply_fusion.1
  3.7 2.5 %keys.1 = bf16[16,128,288]{2,1,0:T(8,128)(2,1)} custom-call(bf16[128,256]{1,0:T(8,128)(2,1)} %bitcast.29, bf16[128,32]{1,0:T(8,128)(2,1)} %bitcast.28, f32[1,256]{1,0:T(1,128)} %bitcast.33, f32[128,32]{1,0:T(8,128)} %get-tuple-element.15.cos_ref, f32[128,32]{1,0:T(8,128)} %get-tuple-element.14.sin_ref), custom_call_target="tpu_custom_call" | custom-call | tf_op jit(solution)/shard_map/keys/pallas_call | solution.py:233
  6.2 0.0 copy-start.1
  6.2 0.0 copy-start.2
  6.2 0.0 copy-start.3
  6.2 0.0 copy-start.5
  6.2 0.0 copy-start.6
  6.2 2.5 %copy.34 = bf16[16,128,288]{1,2,0:T(8,128)(2,1)} copy(bf16[16,128,288]{2,1,0:T(8,128)(2,1)} %keys.1) | data formatting | bytes 2359296 | tf_op jit(solution)/shard_map/keys/pallas_call | solution.py:233
  8.8 8.6 %all-to-all-start = ((bf16[16,128,288]{1,2,0:T(8,128)(2,1)}), bf16[16,128,288]{1,2,0:T(8,128)(2,1)S(1)}, u32[]{:S(2)}, u32[]{:S(2)}) async-start(bf16[16,128,288]{1,2,0:T(8,128)(2,1)} %copy.34), calls=%async_computation | async-start | bytes 2359296 | tf_op jit(solution)/shard_map/all_to_all | solution.py:236
  17.3 0.0 copy-done.1
  17.4 0.7 copy.36.col_ref
  18.1 1.7 routes.1
  19.8 0.0 copy-done.2
  19.8 0.0 copy-done.3
  19.8 0.0 copy-done.5
  19.8 0.0 copy-done.6
  19.8 1.5 sine_multiply_fusion
  21.3 13.5 %all-to-all-done = bf16[16,128,288]{1,2,0:T(8,128)(2,1)S(1)} async-done(((bf16[16,128,288]{1,2,0:T(8,128)(2,1)}), bf16[16,128,288]{1,2,0:T(8,128)(2,1)S(1)}, u32[]{:S(2)}, u32[]{:S(2)}) %all-to-all-start) | async-done | bytes 1179680 | tf_op jit(solution)/shard_map/all_to_all | solution.py:236
  34.8 1.5 copy.35
  36.3 45.8 %attend.1 = (f32[128,2048]{1,0:T(8,128)}, bf16[128,2048]{1,0:T(8,128)(2,1)}, bf16[1024,1024]{1,0:T(8,128)(2,1)}) custom-call(bf16[128,3072]{1,0:T(8,128)(2,1)} %bitcast.24, f32[128,384]{1,0:T(8,128)} %get-tuple-element.13.cos_ref, f32[128,384]{1,0:T(8,128)} %get-tuple-element.12.sin_ref, bf16[2048,288]{1,0:T(8,128)(2,1)} %bitcast.19, ...), custom_call_target="tpu_custom_call" | custom-call | tf_op jit(solution)/shard_map/attend/pallas_call | solution.py:247
  82.1 38.3 %all_to_all.15.rows_ref = bf16[128,8,1024]{2,1,0:T(8,128)(2,1)} all-to-all(bf16[128,8,1024]{2,1,0:T(8,128)(2,1)} %bitcast.23), channel_id=1, replica_groups=mesh['sp'=16,'dp'=8] {'sp','dp'}, dimensions={0} | all-to-all | bytes 4194304 | tf_op jit(solution)/shard_map/all_to_all | solution.py:274
  120.4 14.1 %experts.1 = bf16[128,8,1024]{2,1,0:T(8,128)(2,1)} custom-call(bf16[128,8,1024]{2,1,0:T(8,128)(2,1)} %all_to_all.15.rows_ref, bf16[2048,1024]{1,0:T(8,128)(2,1)} %bitcast.20, bf16[2048,1024]{1,0:T(8,128)(2,1)} %bitcast.21, bf16[1024,2048]{1,0:T(8,128)(2,1)} %bitcast.22), custom_call_target="tpu_custom_call" | custom-call | tf_op jit(solution)/shard_map/experts/pallas_call | solution.py:279
  134.5 0.0 copy-start.4
  134.5 4.5 %all-to-all-start.2 = ((bf16[128,8,1024]{2,1,0:T(8,128)(2,1)}), bf16[128,8,1024]{2,1,0:T(8,128)(2,1)S(1)}, u32[]{:S(2)}, u32[]{:S(2)}) async-start(bf16[128,8,1024]{2,1,0:T(8,128)(2,1)} %experts.1), calls=%async_computation.2 | async-start | bytes 4194304 | tf_op jit(solution)/shard_map/all_to_all | solution.py:294
  139.1 0.0 copy-done.4
  139.1 0.7 copy.37
  139.8 29.9 %all-to-all-done.2 = bf16[128,8,1024]{2,1,0:T(8,128)(2,1)S(1)} async-done(((bf16[128,8,1024]{2,1,0:T(8,128)(2,1)}), bf16[128,8,1024]{2,1,0:T(8,128)(2,1)S(1)}, u32[]{:S(2)}, u32[]{:S(2)}) %all-to-all-start.2) | async-done | bytes 2097184 | tf_op jit(solution)/shard_map/all_to_all | solution.py:294
  169.7 0.0 copy-start
  169.7 1.3 copy-done
  171.0 4.0 %combine.1 = bf16[128,2048]{1,0:T(8,128)(2,1)} custom-call(bf16[1024,1024]{1,0:T(8,128)(2,1)} %bitcast.18, s32[128,2]{1,0:T(8,128)} %get-tuple-element.10.bcol_ref, f32[128,2]{1,0:T(8,128)} %bitcast.27, f32[128,2048]{1,0:T(8,128)} %get-tuple-element.11.mixed_ref), custom_call_target="tpu_custom_call" | custom-call | tf_op jit(solution)/shard_map/combine/pallas_call | solution.py:295
  (1 shorter events, 0.0 us)
Async XLA Ops:
  6.2 11.2 %copy-start.1 = (s32[1,128,2]{1,2,0:T(2,128)S(1)}, s32[1,128,2]{1,2,0:T(2,128)}, u32[]{:S(2)}) copy-start(s32[1,128,2]{1,2,0:T(2,128)} %param.31) | copy-start | bytes 3076
  6.2 13.6 %copy-start.2 = (f32[384]{0:T(512)S(1)}, f32[384]{0:T(512)}, u32[]{:S(2)}) copy-start(f32[384]{0:T(512)} %constant.78) | copy-start | bytes 4612
  6.2 13.6 %copy-start.3 = (f32[384]{0:T(512)S(1)}, f32[384]{0:T(512)}, u32[]{:S(2)}) copy-start(f32[384]{0:T(512)} %constant.79) | copy-start | bytes 4612
  6.2 13.6 %copy-start.5 = (pred[384]{0:T(512)(128)(4,1)S(1)}, pred[384]{0:T(512)(128)(4,1)}, u32[]{:S(2)}) copy-start(pred[384]{0:T(512)(128)(4,1)} %constant.76) | copy-start | bytes 1156
  6.2 13.6 %copy-start.6 = (pred[384]{0:T(512)(128)(4,1)S(1)}, pred[384]{0:T(512)(128)(4,1)}, u32[]{:S(2)}) copy-start(pred[384]{0:T(512)(128)(4,1)} %constant.77) | copy-start | bytes 1156
  8.8 26.0 %all-to-all-start = ((bf16[16,128,288]{1,2,0:T(8,128)(2,1)}), bf16[16,128,288]{1,2,0:T(8,128)(2,1)S(1)}, u32[]{:S(2)}, u32[]{:S(2)}) async-start(bf16[16,128,288]{1,2,0:T(8,128)(2,1)} %copy.34), calls=%async_computation | async-start | bytes 2359296 | tf_op jit(solution)/shard_map/all_to_all | solution.py:236
  134.5 4.6 %copy-start.4 = (f32[1,128,2]{1,2,0:T(2,128)S(1)}, f32[1,128,2]{1,2,0:T(2,128)}, u32[]{:S(2)}) copy-start(f32[1,128,2]{1,2,0:T(2,128)} %param.32) | copy-start | bytes 3076
  134.5 35.1 %all-to-all-start.2 = ((bf16[128,8,1024]{2,1,0:T(8,128)(2,1)}), bf16[128,8,1024]{2,1,0:T(8,128)(2,1)S(1)}, u32[]{:S(2)}, u32[]{:S(2)}) async-start(bf16[128,8,1024]{2,1,0:T(8,128)(2,1)} %experts.1), calls=%async_computation.2 | async-start | bytes 4194304 | tf_op jit(solution)/shard_map/all_to_all | solution.py:294
  169.7 1.3 copy-start

commit v2 on v1

v2 whole, which is shorter than its diff:
```python
import numpy as np
import jax
import jax.numpy as jnp
from jax import lax
from jax.experimental import pallas as pl
from jax.experimental.pallas import tpu as pltpu
from jax.sharding import PartitionSpec as P

D = 2048
HEADS = 32
PLAIN = 64
ROT = 32
QK = PLAIN + ROT
LAT = 256
TOPK = 2
GRID_W = 64
FF = 1024
CAP = 4
GROUP = 4
EPS = 1e-06
CLAMP = 7.0
ALPHA = 1.702
LOG2E = 1.4426950408889634
BF = jnp.bfloat16
F32 = jnp.float32


def prep_kernel(
    off_ref, lat_ref, rope_ref, gain_ref, freq_ref, out_ref, cos_ref, sin_ref
):
    toks = lat_ref.shape[0]
    p = off_ref[0] * toks + lax.broadcasted_iota(jnp.int32, (ROT, toks), 1)
    entry = lax.broadcasted_iota(jnp.int32, (ROT, toks), 0)
    place = jnp.where(entry < ROT // 2, p // GRID_W, p % GRID_W).astype(F32)
    angle = place * freq_ref[...]
    cosine = jnp.cos(angle)
    sine = jnp.where(entry % 2 == 0, -jnp.sin(angle), jnp.sin(angle))
    cos_ref[...] = cosine
    sin_ref[...] = sine
    lat = lat_ref[...].astype(F32)
    ms = jnp.mean(lat * lat, axis=-1, keepdims=True)
    latent = lat * lax.rsqrt(ms + EPS) * gain_ref[...]
    turned = turn(rope_ref[...].astype(F32).T, cosine, sine)
    both = jnp.concatenate([latent.T, turned], axis=0).astype(BF)
    for i in range(out_ref.shape[0]):
        out_ref[i] = both


def turn(x, cosine, sine):
    y = x.reshape(x.shape[0] // 8, 8, x.shape[1])
    even = lax.broadcasted_iota(jnp.int32, y.shape, 1) % 2 == 0
    swapped = jnp.where(even, pltpu.roll(y, 7, 1), pltpu.roll(y, 1, 1)).reshape(x.shape)
    return x * cosine + swapped * sine


def pair_frequencies():
    pair = np.arange(ROT) // 2 % (ROT // 4)
    return (10000.0 ** (-(2.0 * pair) / (ROT // 2))).astype(np.float32)[:, None]


def route_kernel(col_ref, row_ref, weight_ref, bcol_ref, brow_ref, wcol_ref):
    wcol_ref[...] = weight_ref[...]
    n = col_ref.shape[0]
    sub = lax.broadcasted_iota(jnp.int32, (n, n), 0)
    lane = lax.broadcasted_iota(jnp.int32, (n, n), 1)
    e_c = [col_ref[:, k : k + 1] for k in range(2)]
    e_r = [row_ref[k : k + 1, :] for k in range(2)]
    same00 = e_c[0] == e_r[0]
    same11 = e_c[1] == e_r[1]
    one = lambda m: jnp.where(m, 1.0, 0.0)
    r0 = jnp.sum(one(same00 & (lane < sub)), axis=1, keepdims=True)
    r1 = jnp.sum(one(same11 & (lane < sub)), axis=1, keepdims=True) + jnp.sum(
        one(e_c[1] == e_r[0]), axis=1, keepdims=True
    )
    bcol_ref[:, 0:1] = e_c[0] * 8 + r0.astype(jnp.int32)
    bcol_ref[:, 1:2] = e_c[1] * 8 + r1.astype(jnp.int32)
    s0 = jnp.sum(one(same00 & (sub < lane)), axis=0, keepdims=True)
    s1 = jnp.sum(one(same11 & (sub < lane)), axis=0, keepdims=True) + jnp.sum(
        one(e_c[0] == e_r[1]), axis=0, keepdims=True
    )
    brow_ref[0:1, :] = e_r[0] * 8 + s0.astype(jnp.int32)
    brow_ref[1:2, :] = e_r[1] * 8 + s1.astype(jnp.int32)


def dot(a, b, dims):
    return lax.dot_general(a, b, (dims, ((), ())), preferred_element_type=F32)


def attend_kernel(
    q_ref, cos_ref, sin_ref, kt_ref, ku_ref, vup_ref, vuc_ref, wo_ref, res_ref, gain_ref, brow_ref,
    mixed_ref, normed_ref, out_ref,
    keys_ref, klt_ref, bd_ref, qa_ref, qb_ref, sa_ref, sb_ref, pa_ref, pb_ref, mb_ref, heads_ref, acc_ref,
):
    g = pl.program_id(0)
    last = pl.num_programs(0) - 1
    toks = q_ref.shape[0]
    width = 2 * toks
    n_keys = keys_ref.shape[0]
    chunk = 256
    chunks = n_keys // chunk

    @pl.when(g == 0)
    def _():
        for i in range(kt_ref.shape[0]):
            rows = slice(i * toks, (i + 1) * toks)
            klt_ref[:, rows] = kt_ref[i, :LAT, :]
            keys_ref[rows, :] = kt_ref[i].T
        bd_ref[...] = jnp.zeros_like(bd_ref)

    def pieces(x):
        return x.reshape(x.shape[0] // 8, 8, x.shape[1])

    def score_chunk(q, s_ref, i, top):
        rows = slice(i * chunk, (i + 1) * chunk)
        s = dot(keys_ref[rows, :], q, ((1,), (0,)))
        s_ref[rows, :] = s
        part = jnp.max(pieces(s), axis=0)
        return part if top is None else jnp.maximum(top, part)

    def prob_chunk(s_ref, p_ref, i, top, total):
        rows = slice(i * chunk, (i + 1) * chunk)
        p = jnp.exp2(s_ref[rows, :] - top)
        p_ref[rows, :] = p.astype(BF)
        part = jnp.sum(pieces(p), axis=0)
        return part if total is None else total + part

    def heads_of(p_ref, total, vt):
        ctx = dot(klt_ref[...], p_ref[...], ((1,), (0,)))
        inv = 1.0 / jnp.sum(total, axis=0, keepdims=True)
        both = dot(vt, (ctx * inv).astype(BF), ((1,), (0,)))
        return jnp.concatenate([both[:PLAIN, :toks], both[PLAIN:, toks:]], axis=0).astype(BF)

    def project():
        acc_ref[...] += dot(heads_ref[...], wo_ref[...], ((0,), (0,)))

    @pl.when(g < last)
    def _():
        qt = q_ref[...].astype(F32).T * (QK ** -0.5)
        for j in range(GROUP):
            bd_ref[j * PLAIN : (j + 1) * PLAIN, j * toks : (j + 1) * toks] = qt[
                j * QK : j * QK + PLAIN
            ].astype(BF)
        ql = (dot(ku_ref[...], bd_ref[...], ((1,), (0,))) * LOG2E).astype(BF)
        for half, dst in enumerate((qa_ref, qb_ref)):
            dst[:LAT, :] = ql[:, half * width : (half + 1) * width]
            for j in range(2):
                r = (half * 2 + j) * QK + PLAIN
                turned = turn(qt[r : r + ROT], cos_ref[...], sin_ref[...])
                dst[LAT:, j * toks : (j + 1) * toks] = (turned * LOG2E).astype(BF)

        qa = qa_ref[...]
        top, total = None, None
        prev = mb_ref[...]
        for i in range(chunks):
            top = score_chunk(qa, sa_ref, i, top)
            total = prob_chunk(sb_ref, pb_ref, i, prev, total)
        top_a = jnp.max(top, axis=0, keepdims=True)
        heads_ref[width // 2 :, :] = heads_of(pb_ref, total, vup_ref[2 * PLAIN :, :])
        project()
        qb = qb_ref[...]
        top, total = None, None
        for i in range(chunks):
            top = score_chunk(qb, sb_ref, i, top)
            total = prob_chunk(sa_ref, pa_ref, i, top_a, total)
        mb_ref[...] = jnp.max(top, axis=0, keepdims=True)
        heads_ref[: width // 2, :] = heads_of(pa_ref, total, vuc_ref[: 2 * PLAIN, :])

    @pl.when(g == 0)
    def _():
        acc_ref[...] = res_ref[...].astype(F32)

    @pl.when(g == last)
    def _():
        total = None
        prev = mb_ref[...]
        for i in range(chunks):
            total = prob_chunk(sb_ref, pb_ref, i, prev, total)
        heads_ref[width // 2 :, :] = heads_of(pb_ref, total, vup_ref[2 * PLAIN :, :])
        project()
        mixed = acc_ref[...]
        mixed_ref[...] = mixed
        ms = jnp.mean(mixed * mixed, axis=-1, keepdims=True)
        normed = (mixed * lax.rsqrt(ms + EPS) * gain_ref[...]).astype(BF)
        normed_ref[...] = normed
        n_rows = out_ref.shape[0]
        half_d = D // 2
        stacked = jnp.concatenate([normed[:, :half_d], normed[:, half_d:]], axis=0)
        row = lax.broadcasted_iota(jnp.int32, (n_rows, toks), 0)
        picks = []
        for h in range(2):
            m = (row == brow_ref[0:1, :] + 4 * h) | (row == brow_ref[1:2, :] + 4 * h)
            picks.append(jnp.where(m, 1.0, 0.0).astype(BF))
        pick = jnp.concatenate(picks, axis=1)
        out_ref[...] = dot(pick, stacked, ((1,), (0,))).astype(BF)


def expert_kernel(rows_ref, gate_ref, up_ref, lo_ref, hi_ref, out_ref, x_ref, hidden_ref):
    f = pl.program_id(0)
    n_src = rows_ref.shape[0]
    half_d = D // 2
    fb = gate_ref.shape[1]
    f_steps = FF // fb

    @pl.when(f == 0)
    def _():
        r = rows_ref[...].astype(F32).reshape(n_src // 2, 2, 8, half_d)
        a, b = r[:, 0], r[:, 1]
        low = lax.broadcasted_iota(jnp.int32, a.shape, 1) < 4
        first = jnp.where(low, a, pltpu.roll(b, 4, 1))
        second = jnp.where(low, pltpu.roll(a, 4, 1), b)
        x_ref[:, :half_d] = first.reshape(n_src * 4, half_d).astype(BF)
        x_ref[:, half_d:] = second.reshape(n_src * 4, half_d).astype(BF)

    @pl.when(f < f_steps)
    def _():
        x = x_ref[...]
        gate = dot(x, gate_ref[...], ((1,), (0,)))
        up = dot(x, up_ref[...], ((1,), (0,)))
        cut = jnp.minimum(gate, CLAMP)
        act = cut * jax.nn.sigmoid(ALPHA * cut) * (jnp.clip(up, -CLAMP, CLAMP) + 1.0)
        hidden_ref[f] = act.astype(BF)

    @pl.when(f >= f_steps)
    def _():
        hidden = jnp.concatenate([hidden_ref[i] for i in range(f_steps)], axis=1)
        lanes = lo_ref.shape[1]
        lo = dot(hidden, lo_ref[...], ((1,), (0,))).reshape(n_src // 2, 8, lanes)
        hi = dot(hidden, hi_ref[...], ((1,), (0,))).reshape(n_src // 2, 8, lanes)
        low = lax.broadcasted_iota(jnp.int32, lo.shape, 1) < 4
        first = jnp.where(low, lo, pltpu.roll(hi, 4, 1))
        second = jnp.where(low, pltpu.roll(lo, 4, 1), hi)
        both = jnp.concatenate([first[:, None], second[:, None]], axis=1)
        out_ref[...] = both.reshape(n_src, 8, lanes).astype(BF)


def combine_kernel(rows_ref, bcol_ref, weight_ref, mixed_ref, out_ref, pick_ref):
    n = pl.program_id(0)
    n_rows = rows_ref.shape[0]
    toks = mixed_ref.shape[0]
    per = pl.num_programs(0) // 2

    @pl.when(n % per == 0)
    def _():
        lane = lax.broadcasted_iota(jnp.int32, (toks, n_rows), 1)
        shift = 4 * (n // per)
        for k in range(TOPK):
            pick = jnp.where(lane == bcol_ref[:, k : k + 1] + shift, 1.0, 0.0).astype(BF)
            pick_ref[k * toks : (k + 1) * toks, :] = pick

    got = dot(pick_ref[...], rows_ref[...], ((1,), (0,)))
    total = mixed_ref[...]
    for k in range(TOPK):
        total += weight_ref[:, k : k + 1] * got[k * toks : (k + 1) * toks]
    out_ref[...] = total.astype(BF)


def full(*shape):
    return pl.BlockSpec(shape, lambda *_: (0,) * len(shape))


def params(mb=60):
    return pltpu.CompilerParams(vmem_limit_bytes=mb * 1024 * 1024)


def attend(q, ct, st, keys, ku, vut, wo, res, gain, brow, experts):
    sds = jax.ShapeDtypeStruct
    toks = q.shape[0]
    keys_n = keys.shape[0] * toks
    steps = HEADS // GROUP
    now = lambda g: jnp.minimum(g, steps - 1)
    before = lambda g: jnp.maximum(g - 1, 0)
    return pl.pallas_call(
        attend_kernel,
        grid=(steps + 1,),
        in_specs=[
            pl.BlockSpec((toks, GROUP * QK), lambda g: (0, now(g))),
            full(ROT, toks),
            full(ROT, toks),
            full(*keys.shape),
            pl.BlockSpec((LAT, GROUP * PLAIN), lambda g: (0, now(g))),
            pl.BlockSpec((GROUP * PLAIN, LAT), lambda g: (before(g), 0)),
            pl.BlockSpec((GROUP * PLAIN, LAT), lambda g: (now(g), 0)),
            pl.BlockSpec((GROUP * PLAIN, D), lambda g: (before(g), 0)),
            full(toks, D),
            full(1, D),
            full(TOPK, toks),
        ],
        out_specs=(full(toks, D), full(toks, D), full(experts * 8, D // 2)),
        out_shape=(sds((toks, D), F32), sds((toks, D), BF), sds((experts * 8, D // 2), BF)),
        scratch_shapes=[
            pltpu.VMEM((keys_n, LAT + ROT), BF),
            pltpu.VMEM((LAT, keys_n), BF),
            pltpu.VMEM((GROUP * PLAIN, GROUP * toks), BF),
            pltpu.VMEM((LAT + ROT, 2 * toks), BF),
            pltpu.VMEM((LAT + ROT, 2 * toks), BF),
            pltpu.VMEM((keys_n, 2 * toks), F32),
            pltpu.VMEM((keys_n, 2 * toks), F32),
            pltpu.VMEM((keys_n, 2 * toks), BF),
            pltpu.VMEM((keys_n, 2 * toks), BF),
            pltpu.VMEM((1, 2 * toks), F32),
            pltpu.VMEM((GROUP * PLAIN, toks), BF),
            pltpu.VMEM((toks, D), F32),
        ],
        compiler_params=params(),
        name="attend",
    )(q, ct, st, keys, ku, vut, vut, wo, res, gain, brow)


def local(
    queries, kv_latent, rope_key, latent_norm_gain, key_up_weight, value_up_weight, out_proj,
    residual, ffn_gain, routes, route_weights, expert_gate, expert_up, expert_down,
):
    toks = queries.shape[1]
    sp = lax.axis_size("sp")
    experts = sp * lax.axis_size("dp")
    sds = jax.ShapeDtypeStruct
    offset = lax.axis_index("sp").astype(jnp.int32)[None]
    packed, ct, st = pl.pallas_call(
        prep_kernel,
        in_specs=[pl.BlockSpec(memory_space=pltpu.SMEM)] + [pl.BlockSpec()] * 4,
        out_shape=(sds((sp, LAT + ROT, toks), BF), sds((ROT, toks), F32), sds((ROT, toks), F32)),
        compiler_params=params(),
        name="prep",
    )(offset, kv_latent[0], rope_key[0], latent_norm_gain[None], pair_frequencies())
    keys = lax.all_to_all(packed, "sp", 0, 0, tiled=True)
    bcol, brow, wcol = pl.pallas_call(
        route_kernel,
        out_shape=(
            sds((toks, TOPK), jnp.int32), sds((TOPK, toks), jnp.int32), sds((toks, TOPK), F32)
        ),
        compiler_params=params(),
        name="routes",
    )(routes[0], routes[0].T, route_weights[0])

    mixed, normed, outgoing = attend(
        queries[0], ct, st, keys, key_up_weight, value_up_weight.T, out_proj, residual[0],
        ffn_gain[None], brow, experts,
    )

    slot_rows = lax.all_to_all(
        outgoing.reshape(experts, 8, D // 2), ("sp", "dp"), 0, 0, tiled=True
    )
    f_steps, o_steps = 4, 2
    fb, lanes = FF // f_steps, D // 2 // o_steps
    low = lambda f: jnp.minimum(f, f_steps - 1)
    out_at = lambda f: jnp.maximum(f - f_steps, 0)
    expert_out = pl.pallas_call(
        expert_kernel,
        grid=(f_steps + o_steps,),
        in_specs=[
            full(experts, 8, D // 2),
            pl.BlockSpec((D, fb), lambda f: (0, low(f))),
            pl.BlockSpec((D, fb), lambda f: (0, low(f))),
            pl.BlockSpec((FF, lanes), lambda f: (0, out_at(f))),
            pl.BlockSpec((FF, lanes), lambda f: (0, out_at(f) + o_steps)),
        ],
        out_specs=pl.BlockSpec((experts, 8, lanes), lambda f: (0, 0, out_at(f))),
        out_shape=sds((experts, 8, D // 2), BF),
        scratch_shapes=[
            pltpu.VMEM((experts * CAP, D), BF), pltpu.VMEM((f_steps, experts * CAP, fb), BF)
        ],
        compiler_params=params(),
        name="experts",
    )(slot_rows, expert_gate[0], expert_up[0], expert_down[0], expert_down[0])
    returned = lax.all_to_all(expert_out, ("sp", "dp"), 0, 0, tiled=True)
    per = 2
    layer_out = pl.pallas_call(
        combine_kernel,
        grid=(2 * per,),
        in_specs=[
            pl.BlockSpec((experts * 8, D // 2 // per), lambda n: (0, n % per)),
            full(toks, TOPK),
            full(toks, TOPK),
            pl.BlockSpec((toks, D // 2 // per), lambda n: (0, n)),
        ],
        out_specs=pl.BlockSpec((toks, D // 2 // per), lambda n: (0, n)),
        out_shape=sds((toks, D), BF),
        scratch_shapes=[pltpu.VMEM((TOPK * toks, experts * 8), BF)],
        compiler_params=params(),
        name="combine",
    )(returned.reshape(experts * 8, D // 2), bcol, wcol, mixed)
    return normed[None], layer_out[None]


def solution(mesh):
    tok = P("dp", "sp", None)
    exp = P(("sp", "dp"), None, None)
    in_specs = (
        tok, tok, tok, P(), P(), P(), P(), tok, P(), tok, tok, exp, exp, exp,
    )
    return jax.shard_map(
        local, mesh=mesh, in_specs=in_specs, out_specs=(tok, tok), check_vma=False
    )
```

time: 176 us -> 155 us (0.88)
  blocking collectives: 38.3 us -> 74.2 us
  waiting for transfers between devices: 43.3 us -> 12.9 us
  Pallas kernels: 68.1 us -> 52.2 us
  starting transfers between devices: 13.1 us -> 8.59 us
  other arithmetic: 3.2 us -> 0 us
  local copies, waits for them, and re-layouts: 8.31 us -> 5.34 us
    all_to_all x0 -> x1, blocking collectives: none -> 35.9 us  [local(): returned = lax.all_to_all(expert_out, ('sp', 'dp'), 0, 0, tiled=True)]
    all_to_all x2 -> x1, waiting for transfers between devices: 43.3 us -> 12.9 us  [local(): keys = lax.all_to_all(packed, 'sp', 0, 0, tiled=True)]
    pallas_call x4, Pallas kernels: 66.4 us -> 50.5 us  [the longest x1 29.7 us: attend(): pl.pallas_call(attend_kernel, grid=(steps + 1,), in_specs=[pl.BlockSpec((...]
    all_to_all x2 -> x1, starting transfers between devices: 13.1 us -> 8.59 us  [local(): keys = lax.all_to_all(packed, 'sp', 0, 0, tiled=True)]
    mul x2 -> x0, other arithmetic: 3.19 us -> none  [lane_tables(): return (cosine, jnp.sin(angle) * sign[None])]
    pallas_call x1 -> x0, local copies, waits for them, and re-layouts: 2.54 us -> none  [local(): pl.pallas_call(key_kernel, out_shape=sds((sp, toks, LAT + ROT), BF), comp...]
    unnamed x16 -> x11, local copies, waits for them, and re-layouts: 3.49 us -> 4.6 us
  transfers between devices with their start and end apart: 2 -> 1, of which waited for: 2 -> 1; matrix products, arithmetic and copies ran while one was open for 2% -> 2% of each run, Pallas kernels for 1% -> 1%
where the time goes in v2:
time: 155 us; the launch traced here: 154 us
  blocking collectives  74.2 us (48%)
  Pallas kernels  52.2 us (34%)
  waiting for transfers between devices  12.9 us (8%)
  starting transfers between devices  8.59 us (6%)
  local copies, waits for them, and re-layouts  5.34 us (3%)
    all_to_all x1, blocking collectives, local(): lax.all_to_all(outgoing.reshape(experts, 8, D // 2), ('sp', 'dp'), 0, 0,...  38.3 us
    all_to_all x1, blocking collectives, local(): returned = lax.all_to_all(expert_out, ('sp', 'dp'), 0, 0, tiled=True)  35.9 us
    pallas_call x1, Pallas kernels, attend(): pl.pallas_call(attend_kernel, grid=(steps + 1,), in_specs=[pl.BlockSpec((...  29.7 us
    pallas_call x1, Pallas kernels, local(): pl.pallas_call(expert_kernel, grid=(f_steps + o_steps,), in_specs=[full(e...  13.7 us
    all_to_all x1, waiting for transfers between devices, local(): keys = lax.all_to_all(packed, 'sp', 0, 0, tiled=True)  12.9 us
    all_to_all x1, starting transfers between devices, local(): keys = lax.all_to_all(packed, 'sp', 0, 0, tiled=True)  8.59 us
    pallas_call x1, Pallas kernels, local(): pl.pallas_call(combine_kernel, grid=(2 * per,), in_specs=[pl.BlockSpec((e...  4.98 us
    unnamed x11, local copies, waits for them, and re-layouts  4.6 us
  transfers between devices with their start and end apart: 1, of which 1 were waited for; matrix products, arithmetic and copies ran while one was open for 2% of the time, Pallas kernels for 1%

profile of v2, /device:TPU:1, one launch (start us, length us, event | category | flops | bytes accessed | tf_op | source)
XLA Modules:
  0.0 154.0 jit_solution(15219797120931312071)
XLA Ops:
  0.6 0.0 copy-start.3
  0.6 0.0 copy-start.2
  0.7 0.0 copy-start.1
  0.7 1.5 copy.17
  2.2 2.2 %prep.1 = (bf16[16,288,128]{2,1,0:T(8,128)(2,1)}, f32[32,128]{1,0:T(8,128)}, f32[32,128]{1,0:T(8,128)}) custom-call(s32[1]{0:T(128)} %bitcast.1.off_ref, bf16[128,256]{1,0:T(8,128)(2,1)} %bitcast.32, bf16[128,32]{1,0:T(8,128)(2,1)} %bitcast.31, f32[1,256]{1,0:T(1,128)} %bitcast.36, f32[32,1]{1,0:T(8,128)} %constant.8.clone.freq_ref), custom_call_target="tpu_custom_call" | custom-call | tf_op jit(solution)/shard_map/prep/pallas_call | solution.py:318
  4.3 8.6 %all-to-all-start = ((bf16[16,288,128]{2,1,0:T(8,128)(2,1)}), bf16[16,288,128]{2,1,0:T(8,128)(2,1)S(1)}, u32[]{:S(2)}, u32[]{:S(2)}) async-start(bf16[16,288,128]{2,1,0:T(8,128)(2,1)} %get-tuple-element.13), calls=%async_computation | async-start | bytes 2359296 | tf_op jit(solution)/shard_map/all_to_all | solution.py:325
  12.9 0.0 copy-done.3
  12.9 0.7 copy.19
  13.7 0.0 copy-done.2
  13.7 0.7 copy.20.col_ref
  14.4 0.0 copy-done.1
  14.4 1.3 copy.18
  15.8 1.7 %routes.1 = (s32[128,2]{1,0:T(8,128)}, s32[2,128]{1,0:T(2,128)}, f32[128,2]{1,0:T(8,128)}) custom-call(s32[128,2]{1,0:T(8,128)} %copy.20.col_ref, s32[2,128]{1,0:T(2,128)} %bitcast.34, f32[128,2]{1,0:T(8,128)} %bitcast.30), custom_call_target="tpu_custom_call" | custom-call | tf_op jit(solution)/shard_map/routes/pallas_call | solution.py:326
  17.5 12.9 %all-to-all-done.kt_ref = bf16[16,288,128]{2,1,0:T(8,128)(2,1)S(1)} async-done(((bf16[16,288,128]{2,1,0:T(8,128)(2,1)}), bf16[16,288,128]{2,1,0:T(8,128)(2,1)S(1)}, u32[]{:S(2)}, u32[]{:S(2)}) %all-to-all-start) | async-done | bytes 1179680 | tf_op jit(solution)/shard_map/all_to_all | solution.py:325
  30.4 0.0 copy-start
  30.4 1.0 copy-done
  31.4 29.7 %attend.1 = (f32[128,2048]{1,0:T(8,128)}, bf16[128,2048]{1,0:T(8,128)(2,1)}, bf16[1024,1024]{1,0:T(8,128)(2,1)}) custom-call(bf16[128,3072]{1,0:T(8,128)(2,1)} %bitcast.27, f32[32,128]{1,0:T(8,128)} %get-tuple-element.11.cos_ref, f32[32,128]{1,0:T(8,128)} %get-tuple-element.12.sin_ref, bf16[16,288,128]{2,1,0:T(8,128)(2,1)} %copy-done, ...), custom_call_target="tpu_custom_call" | custom-call | tf_op jit(solution)/shard_map/attend/pallas_call | solution.py:272
  61.1 38.3 %all_to_all.15.rows_ref = bf16[128,8,1024]{2,1,0:T(8,128)(2,1)} all-to-all(bf16[128,8,1024]{2,1,0:T(8,128)(2,1)} %bitcast.26), channel_id=1, replica_groups=mesh['sp'=16,'dp'=8] {'sp','dp'}, dimensions={0} | all-to-all | bytes 4194304 | tf_op jit(solution)/shard_map/all_to_all | solution.py:340
  99.4 13.7 %experts.1 = bf16[128,8,1024]{2,1,0:T(8,128)(2,1)} custom-call(bf16[128,8,1024]{2,1,0:T(8,128)(2,1)} %all_to_all.15.rows_ref, bf16[2048,1024]{1,0:T(8,128)(2,1)} %bitcast.24, bf16[2048,1024]{1,0:T(8,128)(2,1)} %bitcast.25, bf16[1024,2048]{1,0:T(8,128)(2,1)} %bitcast.19, bf16[1024,2048]{1,0:T(8,128)(2,1)} %bitcast.20), custom_call_target="tpu_custom_call" | custom-call | tf_op jit(solution)/shard_map/experts/pallas_call | solution.py:347
  113.1 35.9 %all_to_all.16 = bf16[128,8,1024]{2,1,0:T(8,128)(2,1)} all-to-all(bf16[128,8,1024]{2,1,0:T(8,128)(2,1)} %experts.1), channel_id=1, replica_groups=mesh['sp'=16,'dp'=8] {'sp','dp'}, dimensions={0} | all-to-all | bytes 4194304 | tf_op jit(solution)/shard_map/all_to_all | solution.py:365
  149.0 5.0 %combine.1 = bf16[128,2048]{1,0:T(8,128)(2,1)} custom-call(bf16[1024,1024]{1,0:T(8,128)(2,1)} %bitcast.23, s32[128,2]{1,0:T(8,128)} %get-tuple-element.17.bcol_ref, f32[128,2]{1,0:T(8,128)} %get-tuple-element.18.weight_ref, f32[128,2048]{1,0:T(8,128)} %get-tuple-element.19.mixed_ref), custom_call_target="tpu_custom_call" | custom-call | tf_op jit(solution)/shard_map/combine/pallas_call | solution.py:367
Async XLA Ops:
  0.6 12.3 %copy-start.3 = (f32[1,128,2]{1,2,0:T(2,128)S(1)}, f32[1,128,2]{1,2,0:T(2,128)}, u32[]{:S(2)}) copy-start(f32[1,128,2]{1,2,0:T(2,128)} %param.25) | copy-start | bytes 3076
  0.6 13.0 %copy-start.2 = (s32[1,128,2]{1,2,0:T(2,128)S(1)}, s32[1,128,2]{1,2,0:T(2,128)}, u32[]{:S(2)}) copy-start(s32[1,128,2]{1,2,0:T(2,128)} %param.24) | copy-start | bytes 3076
  0.7 13.8 %copy-start.1 = (bf16[256,2048]{1,0:T(8,128)(2,1)S(1)}, bf16[256,2048]{1,0:T(8,128)(2,1)}, u32[]{:S(2)}) copy-start(bf16[256,2048]{1,0:T(8,128)(2,1)} %param.20) | copy-start | bytes 3145732
  4.3 26.0 %all-to-all-start = ((bf16[16,288,128]{2,1,0:T(8,128)(2,1)}), bf16[16,288,128]{2,1,0:T(8,128)(2,1)S(1)}, u32[]{:S(2)}, u32[]{:S(2)}) async-start(bf16[16,288,128]{2,1,0:T(8,128)(2,1)} %get-tuple-element.13), calls=%async_computation | async-start | bytes 2359296 | tf_op jit(solution)/shard_map/all_to_all | solution.py:325
  30.4 1.0 copy-start

commit v3 on v2

v3 whole, which is shorter than its diff:
```python
import numpy as np
import jax
import jax.numpy as jnp
from jax import lax
from jax.experimental import pallas as pl
from jax.experimental.pallas import tpu as pltpu
from jax.sharding import PartitionSpec as P

D = 2048
HEADS = 32
PLAIN = 64
ROT = 32
QK = PLAIN + ROT
LAT = 256
TOPK = 2
GRID_W = 64
FF = 1024
CAP = 4
GROUP = 4
CHUNK = 256
EPS = 1e-06
CLAMP = 7.0
ALPHA = 1.702
LOG2E = 1.4426950408889634
BF = jnp.bfloat16
F32 = jnp.float32


def prep_kernel(
    off_ref, lat_ref, rope_ref, gain_ref, freq_ref, out_ref, cos_ref, sin_ref
):
    toks = lat_ref.shape[0]
    p = off_ref[0] * toks + lax.broadcasted_iota(jnp.int32, (ROT, toks), 1)
    entry = lax.broadcasted_iota(jnp.int32, (ROT, toks), 0)
    place = jnp.where(entry < ROT // 2, p // GRID_W, p % GRID_W).astype(F32)
    angle = place * freq_ref[...]
    cosine = jnp.cos(angle)
    sine = jnp.where(entry % 2 == 0, -jnp.sin(angle), jnp.sin(angle))
    cos_ref[...] = cosine
    sin_ref[...] = sine
    lat = lat_ref[...].astype(F32)
    ms = jnp.mean(lat * lat, axis=-1, keepdims=True)
    latent = lat * lax.rsqrt(ms + EPS) * gain_ref[...]
    turned = turn(rope_ref[...].astype(F32), cosine, sine)
    both = jnp.concatenate([latent.T, turned], axis=0).astype(BF)
    for i in range(out_ref.shape[0]):
        out_ref[i] = both


def turn(x, cosine, sine):
    y = x.reshape(x.shape[0] // 8, 8, x.shape[1])
    even = lax.broadcasted_iota(jnp.int32, y.shape, 1) % 2 == 0
    swapped = jnp.where(even, pltpu.roll(y, 7, 1), pltpu.roll(y, 1, 1)).reshape(x.shape)
    return x * cosine + swapped * sine


def pair_frequencies():
    pair = np.arange(ROT) // 2 % (ROT // 4)
    return (10000.0 ** (-(2.0 * pair) / (ROT // 2))).astype(np.float32)[:, None]


def route_kernel(col_ref, row_ref, weight_ref, bcol_ref, brow_ref, wcol_ref):
    wcol_ref[...] = weight_ref[...]
    n = col_ref.shape[0]
    sub = lax.broadcasted_iota(jnp.int32, (n, n), 0)
    lane = lax.broadcasted_iota(jnp.int32, (n, n), 1)
    e_c = [col_ref[:, k : k + 1] for k in range(2)]
    e_r = [row_ref[k : k + 1, :] for k in range(2)]
    same00 = e_c[0] == e_r[0]
    same11 = e_c[1] == e_r[1]
    one = lambda m: jnp.where(m, 1.0, 0.0)
    r0 = jnp.sum(one(same00 & (lane < sub)), axis=1, keepdims=True)
    r1 = jnp.sum(one(same11 & (lane < sub)), axis=1, keepdims=True) + jnp.sum(
        one(e_c[1] == e_r[0]), axis=1, keepdims=True
    )
    bcol_ref[:, 0:1] = e_c[0] * 8 + r0.astype(jnp.int32)
    bcol_ref[:, 1:2] = e_c[1] * 8 + r1.astype(jnp.int32)
    s0 = jnp.sum(one(same00 & (sub < lane)), axis=0, keepdims=True)
    s1 = jnp.sum(one(same11 & (sub < lane)), axis=0, keepdims=True) + jnp.sum(
        one(e_c[0] == e_r[1]), axis=0, keepdims=True
    )
    brow_ref[0:1, :] = e_r[0] * 8 + s0.astype(jnp.int32)
    brow_ref[1:2, :] = e_r[1] * 8 + s1.astype(jnp.int32)


def dot(a, b, dims):
    return lax.dot_general(a, b, (dims, ((), ())), preferred_element_type=F32)


def query_kernel(q_ref, cos_ref, sin_ref, ku_ref, out_ref, bd_ref):
    toks = q_ref.shape[0]

    @pl.when(pl.program_id(0) == 0)
    def _():
        bd_ref[...] = jnp.zeros_like(bd_ref)

    qt = q_ref[...].astype(F32).T * (QK ** -0.5)
    for j in range(GROUP):
        bd_ref[j * PLAIN : (j + 1) * PLAIN, j * toks : (j + 1) * toks] = qt[
            j * QK : j * QK + PLAIN
        ].astype(BF)
    out_ref[0, :LAT, :] = (dot(ku_ref[...], bd_ref[...], ((1,), (0,))) * LOG2E).astype(BF)
    for j in range(GROUP):
        r = j * QK + PLAIN
        turned = turn(qt[r : r + ROT], cos_ref[...], sin_ref[...])
        out_ref[0, LAT:, j * toks : (j + 1) * toks] = (turned * LOG2E).astype(BF)


def attend_kernel(
    kt_ref, q0_ref, qb_ref, qa_ref, vb_ref, va_ref, vl_ref, wb_ref, wa_ref, wl_ref, res_ref,
    gain_ref, brow_ref, mixed_ref, normed_ref, out_ref,
    keys_ref, klt_ref, sa_ref, sb_ref, pa_ref, pb_ref, ta_ref, lb_ref, acc_ref,
):
    g = pl.program_id(0)
    last = pl.num_programs(0) - 1
    toks = res_ref.shape[0]
    n_keys = keys_ref.shape[0]
    chunk = CHUNK
    chunks = n_keys // chunk

    def pieces(x):
        return x.reshape(x.shape[0] // 8, 8, x.shape[1])

    def score_chunk(q, s_ref, i, top):
        rows = slice(i * chunk, (i + 1) * chunk)
        s = dot(keys_ref[rows, :], q, ((1,), (0,)))
        s_ref[rows, :] = s
        part = jnp.max(pieces(s), axis=0)
        return part if top is None else jnp.maximum(top, part)

    def prob_chunk(s_ref, p_ref, i, top, total):
        rows = slice(i * chunk, (i + 1) * chunk)
        p = jnp.exp2(s_ref[rows, :] - top)
        p_ref[rows, :] = p.astype(BF)
        part = jnp.sum(pieces(p), axis=0)
        return part if total is None else total + part

    def context(p_ref, total):
        ctx = dot(klt_ref[...], p_ref[...], ((1,), (0,)))
        return (ctx * (1.0 / jnp.sum(total, axis=0, keepdims=True))).astype(BF)

    def heads_of(ctx, vt):
        full_out = dot(vt, ctx, ((1,), (0,)))
        own = [
            full_out[j * PLAIN : (j + 1) * PLAIN, j * toks : (j + 1) * toks] for j in range(GROUP)
        ]
        return jnp.concatenate(own, axis=0).astype(BF)

    def project(heads, w_ref):
        acc_ref[...] += dot(heads, w_ref[...], ((0,), (0,)))

    def stage(q_ref, s_new, s_old, p_new, p_old, top_old, total_old, v_ref, w_ref):
        top, total, ctx, heads = None, None, None, None
        for i in range(chunks):
            if q_ref is not None:
                top = score_chunk(q_ref[0], s_new, i, top)
            total = prob_chunk(s_old, p_new, i, top_old, total)
            if i == chunks // 8:
                ctx = context(p_old, total_old)
            if i == chunks // 2:
                heads = heads_of(ctx, v_ref[...])
            if i == chunks * 3 // 4:
                project(heads, w_ref)
        if q_ref is not None:
            top = jnp.max(top, axis=0, keepdims=True)
        return top, total

    @pl.when(g == 0)
    def _():
        for i in range(kt_ref.shape[0]):
            rows = slice(i * toks, (i + 1) * toks)
            klt_ref[:, rows] = kt_ref[i, :LAT, :]
            keys_ref[rows, :] = kt_ref[i].T
        top = None
        for i in range(chunks):
            top = score_chunk(q0_ref[0], sa_ref, i, top)
        ta_ref[...] = jnp.max(top, axis=0, keepdims=True)

    top_b, total_a = stage(
        qb_ref, sb_ref, sa_ref, pa_ref, pb_ref, ta_ref[...], lb_ref[...], vb_ref, wb_ref
    )

    @pl.when(g == 0)
    def _():
        acc_ref[...] = res_ref[...].astype(F32)

    @pl.when(g < last)
    def _():
        top_a, total_b = stage(
            qa_ref, sa_ref, sb_ref, pb_ref, pa_ref, top_b, total_a, va_ref, wa_ref
        )
        ta_ref[...] = top_a
        lb_ref[...] = total_b

    @pl.when(g == last)
    def _():
        _, total_b = stage(
            None, sa_ref, sb_ref, pb_ref, pa_ref, top_b, total_a, va_ref, wa_ref
        )
        project(heads_of(context(pb_ref, total_b), vl_ref[...]), wl_ref)
        mixed = acc_ref[...]
        mixed_ref[...] = mixed
        ms = jnp.mean(mixed * mixed, axis=-1, keepdims=True)
        normed = (mixed * lax.rsqrt(ms + EPS) * gain_ref[...]).astype(BF)
        normed_ref[...] = normed
        n_rows = out_ref.shape[0]
        half_d = D // 2
        stacked = jnp.concatenate([normed[:, :half_d], normed[:, half_d:]], axis=0)
        row = lax.broadcasted_iota(jnp.int32, (n_rows, toks), 0)
        picks = []
        for h in range(2):
            m = (row == brow_ref[0:1, :] + 4 * h) | (row == brow_ref[1:2, :] + 4 * h)
            picks.append(jnp.where(m, 1.0, 0.0).astype(BF))
        pick = jnp.concatenate(picks, axis=1)
        out_ref[...] = dot(pick, stacked, ((1,), (0,))).astype(BF)


def expert_kernel(
    rows_ref, gate_ref, up_hbm, down_hbm, out_ref, x_ref, hidden_ref, up_ref, down_ref, sem_ref
):
    f = pl.program_id(0)
    copy_up = pltpu.make_async_copy(up_hbm, up_ref, sem_ref.at[0])
    copy_down = pltpu.make_async_copy(down_hbm, down_ref, sem_ref.at[1])
    n_src = rows_ref.shape[0]
    half_d = D // 2
    f_steps, _, fb = hidden_ref.shape
    lanes = out_ref.shape[2]

    @pl.when(f == 0)
    def _():
        copy_up.start()
        copy_down.start()
        r = rows_ref[...].astype(F32).reshape(n_src // 2, 2, 8, half_d)
        a, b = r[:, 0], r[:, 1]
        low = lax.broadcasted_iota(jnp.int32, a.shape, 1) < 4
        first = jnp.where(low, a, pltpu.roll(b, 4, 1))
        second = jnp.where(low, pltpu.roll(a, 4, 1), b)
        x_ref[:, :half_d] = first.reshape(n_src * 4, half_d).astype(BF)
        x_ref[:, half_d:] = second.reshape(n_src * 4, half_d).astype(BF)

    @pl.when(f == 0)
    def _():
        copy_up.wait()

    @pl.when(f == f_steps)
    def _():
        copy_down.wait()

    @pl.when(f < f_steps)
    def _():
        x = x_ref[...]
        cols = pl.ds(pl.multiple_of(f * fb, fb), fb)
        gate = dot(x, gate_ref[:, cols], ((1,), (0,)))
        up = dot(x, up_ref[:, cols], ((1,), (0,)))
        cut = jnp.minimum(gate, CLAMP)
        act = cut * jax.nn.sigmoid(ALPHA * cut) * (jnp.clip(up, -CLAMP, CLAMP) + 1.0)
        hidden_ref[f] = act.astype(BF)

    @pl.when(f >= f_steps)
    def _():
        hidden = jnp.concatenate([hidden_ref[i] for i in range(f_steps)], axis=1)
        at = pl.multiple_of((f - f_steps) * lanes, lanes)
        lo = dot(hidden, down_ref[:, pl.ds(at, lanes)], ((1,), (0,)))
        hi = dot(hidden, down_ref[:, pl.ds(at + half_d, lanes)], ((1,), (0,)))
        lo = lo.reshape(n_src // 2, 8, lanes)
        hi = hi.reshape(n_src // 2, 8, lanes)
        low = lax.broadcasted_iota(jnp.int32, lo.shape, 1) < 4
        first = jnp.where(low, lo, pltpu.roll(hi, 4, 1))
        second = jnp.where(low, pltpu.roll(lo, 4, 1), hi)
        both = jnp.concatenate([first[:, None], second[:, None]], axis=1)
        out_ref[...] = both.reshape(n_src, 8, lanes).astype(BF)


def combine_kernel(rows_ref, bcol_ref, weight_ref, mixed_ref, out_ref, pick_ref):
    n = pl.program_id(0)
    n_rows = rows_ref.shape[0]
    toks = mixed_ref.shape[0]
    per = pl.num_programs(0) // 2

    @pl.when(n % per == 0)
    def _():
        lane = lax.broadcasted_iota(jnp.int32, (toks, n_rows), 1)
        shift = 4 * (n // per)
        for k in range(TOPK):
            pick = jnp.where(lane == bcol_ref[:, k : k + 1] + shift, 1.0, 0.0).astype(BF)
            pick_ref[k * toks : (k + 1) * toks, :] = pick

    lanes = mixed_ref.shape[1]
    cols = pl.ds(pl.multiple_of(n % per * lanes, lanes), lanes)
    got = dot(pick_ref[...], rows_ref[:, cols], ((1,), (0,)))
    total = mixed_ref[...]
    for k in range(TOPK):
        total += weight_ref[:, k : k + 1] * got[k * toks : (k + 1) * toks]
    out_ref[...] = total.astype(BF)


def in_vmem(x):
    return pltpu.with_memory_space_constraint(x, pltpu.VMEM)


def in_hbm(x):
    return pltpu.with_memory_space_constraint(x, pltpu.HBM)


def whole():
    return pl.BlockSpec(memory_space=pltpu.VMEM)


def full(*shape):
    return pl.BlockSpec(shape, lambda *_: (0,) * len(shape))


def params(mb=60):
    return pltpu.CompilerParams(vmem_limit_bytes=mb * 1024 * 1024)


def ready_queries(q, ct, st, ku):
    toks = q.shape[0]
    return pl.pallas_call(
        query_kernel,
        grid=(HEADS // GROUP,),
        in_specs=[
            pl.BlockSpec((toks, GROUP * QK), lambda g: (0, g)),
            full(ROT, toks),
            full(ROT, toks),
            pl.BlockSpec((LAT, GROUP * PLAIN), lambda g: (0, g)),
        ],
        out_specs=pl.BlockSpec((1, LAT + ROT, GROUP * toks), lambda g: (g, 0, 0)),
        out_shape=jax.ShapeDtypeStruct((HEADS // GROUP, LAT + ROT, GROUP * toks), BF),
        scratch_shapes=[pltpu.VMEM((GROUP * PLAIN, GROUP * toks), BF)],
        compiler_params=params(24),
        name="queries",
    )(q, ct, st, ku)


def attend(qs, keys, vut, wo, res, gain, brow, experts):
    sds = jax.ShapeDtypeStruct
    toks = res.shape[0]
    keys_n = keys.shape[0] * toks
    groups = HEADS // GROUP
    before = lambda g: jnp.maximum(2 * g - 1, 0)
    q_at = lambda f: pl.BlockSpec((1, LAT + ROT, GROUP * toks), lambda g: (f(g), 0, 0))
    v_at = lambda f: pl.BlockSpec((GROUP * PLAIN, LAT), lambda g: (f(g), 0))
    w_at = lambda f: pl.BlockSpec((GROUP * PLAIN, D), lambda g: (f(g), 0))
    return pl.pallas_call(
        attend_kernel,
        grid=(groups // 2,),
        in_specs=[
            whole(),
            q_at(lambda g: 0),
            q_at(lambda g: 2 * g + 1),
            q_at(lambda g: jnp.minimum(2 * g + 2, groups - 1)),
            v_at(before),
            v_at(lambda g: 2 * g),
            v_at(lambda g: groups - 1),
            w_at(before),
            w_at(lambda g: 2 * g),
            w_at(lambda g: groups - 1),
            full(toks, D),
            full(1, D),
            full(TOPK, toks),
        ],
        out_specs=(full(toks, D), full(toks, D), full(experts * 8, D // 2)),
        out_shape=(sds((toks, D), F32), sds((toks, D), BF), sds((experts * 8, D // 2), BF)),
        scratch_shapes=[
            pltpu.VMEM((keys_n, LAT + ROT), BF),
            pltpu.VMEM((LAT, keys_n), BF),
            pltpu.VMEM((keys_n, GROUP * toks), F32),
            pltpu.VMEM((keys_n, GROUP * toks), F32),
            pltpu.VMEM((keys_n, GROUP * toks), BF),
            pltpu.VMEM((keys_n, GROUP * toks), BF),
            pltpu.VMEM((1, GROUP * toks), F32),
            pltpu.VMEM((8, GROUP * toks), F32),
            pltpu.VMEM((toks, D), F32),
        ],
        compiler_params=params(44),
        name="attend",
    )(keys, qs, qs, qs, vut, vut, vut, wo, wo, wo, res, gain, brow)


def local(
    queries, kv_latent, rope_key, latent_norm_gain, key_up_weight, value_up_weight, out_proj,
    residual, ffn_gain, routes, route_weights, expert_gate, expert_up, expert_down,
):
    toks = queries.shape[1]
    sp = lax.axis_size("sp")
    experts = sp * lax.axis_size("dp")
    sds = jax.ShapeDtypeStruct
    offset = lax.axis_index("sp").astype(jnp.int32)[None]
    packed, ct, st = pl.pallas_call(
        prep_kernel,
        in_specs=[pl.BlockSpec(memory_space=pltpu.SMEM)] + [pl.BlockSpec()] * 4,
        out_shape=(sds((sp, LAT + ROT, toks), BF), sds((ROT, toks), F32), sds((ROT, toks), F32)),
        compiler_params=params(),
        name="prep",
    )(offset, kv_latent[0], rope_key[0].T, latent_norm_gain[None], pair_frequencies())
    keys = in_vmem(lax.all_to_all(packed, "sp", 0, 0, tiled=True))
    bcol, brow, wcol = pl.pallas_call(
        route_kernel,
        out_shape=(
            sds((toks, TOPK), jnp.int32), sds((TOPK, toks), jnp.int32), sds((toks, TOPK), F32)
        ),
        compiler_params=params(),
        name="routes",
    )(routes[0], routes[0].T, route_weights[0])

    mixed, normed, outgoing = attend(
        ready_queries(queries[0], ct, st, key_up_weight), keys, value_up_weight.T, out_proj,
        in_hbm(residual[0]), ffn_gain[None], brow, experts,
    )

    slot_rows = lax.all_to_all(
        outgoing.reshape(experts, 8, D // 2), ("sp", "dp"), 0, 0, tiled=True
    )
    f_steps, o_steps = 4, 2
    fb, lanes = FF // f_steps, D // 2 // o_steps
    out_at = lambda f: jnp.maximum(f - f_steps, 0)
    expert_out = pl.pallas_call(
        expert_kernel,
        grid=(f_steps + o_steps,),
        in_specs=[whole()] * 2 + [pl.BlockSpec(memory_space=pl.ANY)] * 2,
        out_specs=pl.BlockSpec((experts, 8, lanes), lambda f: (0, 0, out_at(f))),
        out_shape=sds((experts, 8, D // 2), BF),
        scratch_shapes=[
            pltpu.VMEM((experts * CAP, D), BF),
            pltpu.VMEM((f_steps, experts * CAP, fb), BF),
            pltpu.VMEM((D, FF), BF),
            pltpu.VMEM((FF, D), BF),
            pltpu.SemaphoreType.DMA((2,)),
        ],
        compiler_params=params(40),
        name="experts",
    )(
        in_vmem(slot_rows),
        in_vmem(expert_gate[0]),
        expert_up[0],
        expert_down[0],
    )
    returned = lax.all_to_all(expert_out, ("sp", "dp"), 0, 0, tiled=True)
    per = 2
    layer_out = pl.pallas_call(
        combine_kernel,
        grid=(2 * per,),
        in_specs=[
            whole(),
            full(toks, TOPK),
            full(toks, TOPK),
            pl.BlockSpec((toks, D // 2 // per), lambda n: (0, n)),
        ],
        out_specs=pl.BlockSpec((toks, D // 2 // per), lambda n: (0, n)),
        out_shape=sds((toks, D), BF),
        scratch_shapes=[pltpu.VMEM((TOPK * toks, experts * 8), BF)],
        compiler_params=params(40),
        name="combine",
    )(in_vmem(returned.reshape(experts * 8, D // 2)), bcol, wcol, mixed)
    return normed[None], layer_out[None]


def solution(mesh):
    tok = P("dp", "sp", None)
    exp = P(("sp", "dp"), None, None)
    in_specs = (
        tok, tok, tok, P(), P(), P(), P(), tok, P(), tok, tok, exp, exp, exp,
    )
    return jax.shard_map(
        local, mesh=mesh, in_specs=in_specs, out_specs=(tok, tok), check_vma=False
    )
```

time: 155 us -> 137 us (0.88)
  Pallas kernels: 52.2 us -> 41.8 us
  waiting for transfers between devices: 12.9 us -> 8.38 us
  blocking collectives: 74.2 us -> 72.5 us
    pallas_call x3 -> x4, Pallas kernels: 48.4 us -> 37.9 us  [the longest x1 22.7 us: attend(): pl.pallas_call(attend_kernel, grid=(groups // 2,), in_specs=[whole(), q_a...]
    all_to_all x1, waiting for transfers between devices: 12.9 us -> 8.38 us  [local(): keys = in_vmem(lax.all_to_all(packed, 'sp', 0, 0, tiled=True))]
    unnamed x11 -> x28, local copies, waits for them, and re-layouts: 4.6 us -> 3.66 us
  transfers between devices with their start and end apart: 1 -> 1, of which waited for: 1 -> 1; matrix products, arithmetic and copies ran while one was open for 2% -> 1% of each run, Pallas kernels for 1% -> 3%
where the time goes in v3:
time: 137 us
  blocking collectives  72.5 us (53%)
  Pallas kernels  41.8 us (31%)
  starting transfers between devices  8.76 us (6%)
  waiting for transfers between devices  8.38 us (6%)
  local copies, waits for them, and re-layouts  4.4 us (3%)
    all_to_all x1, blocking collectives, local(): lax.all_to_all(outgoing.reshape(experts, 8, D // 2), ('sp', 'dp'), 0, 0,...  38 us
    all_to_all x1, blocking collectives, local(): returned = lax.all_to_all(expert_out, ('sp', 'dp'), 0, 0, tiled=True)  34.5 us
    pallas_call x1, Pallas kernels, attend(): pl.pallas_call(attend_kernel, grid=(groups // 2,), in_specs=[whole(), q_a...  22.7 us
    pallas_call x1, Pallas kernels, local(): pl.pallas_call(expert_kernel, grid=(f_steps + o_steps,), in_specs=[whole(...  9.03 us
    all_to_all x1, starting transfers between devices, local(): keys = in_vmem(lax.all_to_all(packed, 'sp', 0, 0, tiled=True))  8.76 us
    all_to_all x1, waiting for transfers between devices, local(): keys = in_vmem(lax.all_to_all(packed, 'sp', 0, 0, tiled=True))  8.38 us
    unnamed x28, local copies, waits for them, and re-layouts  3.66 us
    pallas_call x1, Pallas kernels, local(): pl.pallas_call(combine_kernel, grid=(2 * per,), in_specs=[whole(), full(t...  3.07 us
  transfers between devices with their start and end apart: 1, of which 1 were waited for; matrix products, arithmetic and copies ran while one was open for 1% of the time, Pallas kernels for 3%

profile of v3, /device:TPU:1, one launch (start us, length us, event | category | flops | bytes accessed | tf_op | source)
XLA Modules:
  0.0 136.6 jit_solution(14022142553691631691)
XLA Ops:
  0.6 0.0 copy-start.12
  0.6 0.0 copy-start.11
  0.7 0.0 copy-start.10
  0.7 2.2 %prep.1 = (bf16[16,288,128]{2,1,0:T(8,128)(2,1)}, f32[32,128]{1,0:T(8,128)}, f32[32,128]{1,0:T(8,128)}) custom-call(s32[1]{0:T(128)} %bitcast.off_ref, bf16[128,256]{1,0:T(8,128)(2,1)} %bitcast.34, bf16[32,128]{1,0:T(8,128)(2,1)} %bitcast.35, f32[1,256]{1,0:T(1,128)} %bitcast.38, f32[32,1]{1,0:T(8,128)} %constant.8.clone.freq_ref), custom_call_target="tpu_custom_call" | custom-call | tf_op jit(solution)/shard_map/prep/pallas_call | solution.py:390
  2.9 0.0 copy-start.6
  2.9 0.0 copy-start.7
  2.9 8.8 %all-to-all-start = ((bf16[16,288,128]{2,1,0:T(8,128)(2,1)}), bf16[16,288,128]{2,1,0:T(8,128)(2,1)}, u32[]{:S(2)}, u32[]{:S(2)}) async-start(bf16[16,288,128]{2,1,0:T(8,128)(2,1)} %get-tuple-element.11), calls=%async_computation | async-start | bytes 2359296 | tf_op jit(solution)/shard_map/all_to_all | solution.py:397
  11.7 0.0 copy-done.12
  11.7 0.7 copy.18
  12.4 0.0 copy-done.11
  12.4 0.7 copy.19.col_ref
  13.2 0.0 copy-done.10
  13.2 0.5 copy.17
  13.7 1.7 %routes.1 = (s32[128,2]{1,0:T(8,128)}, s32[2,128]{1,0:T(2,128)}, f32[128,2]{1,0:T(8,128)}) custom-call(s32[128,2]{1,0:T(8,128)} %copy.19.col_ref, s32[2,128]{1,0:T(2,128)} %bitcast.36, f32[128,2]{1,0:T(8,128)} %bitcast.33), custom_call_target="tpu_custom_call" | custom-call | tf_op jit(solution)/shard_map/routes/pallas_call | solution.py:398
  15.4 0.0 copy-done.6
  15.4 0.0 copy-done.7
  15.4 0.0 copy-start.2
  15.4 1.2 copy-done.2
  16.6 0.0 copy-start.3
  16.7 1.1 copy-done.3
  17.8 0.0 copy-start.8
  17.8 0.0 copy-start.9
  17.8 3.0 %queries.1.q0_ref.qb_ref.qa_ref = bf16[8,288,512]{2,1,0:T(8,128)(2,1)S(1)} custom-call(bf16[128,3072]{1,0:T(8,128)(2,1)S(1)} %bitcast.28, f32[32,128]{1,0:T(8,128)S(1)} %copy-done.6, f32[32,128]{1,0:T(8,128)S(1)} %copy-done.7, bf16[256,2048]{1,0:T(8,128)(2,1)S(1)} %copy-done.2), custom_call_target="tpu_custom_call" | custom-call | tf_op jit(solution)/shard_map/queries/pallas_call | solution.py:319
  20.8 8.4 %all-to-all-done.kt_ref = bf16[16,288,128]{2,1,0:T(8,128)(2,1)} async-done(((bf16[16,288,128]{2,1,0:T(8,128)(2,1)}), bf16[16,288,128]{2,1,0:T(8,128)(2,1)}, u32[]{:S(2)}, u32[]{:S(2)}) %all-to-all-start) | async-done | bytes 1179680 | tf_op jit(solution)/shard_map/all_to_all | solution.py:397
  29.2 0.0 copy-done.8
  29.2 0.0 copy-done.9
  29.2 0.0 copy-start.1
  29.2 22.7 %attend.1 = (f32[128,2048]{1,0:T(8,128)S(1)}, bf16[128,2048]{1,0:T(8,128)(2,1)}, bf16[1024,1024]{1,0:T(8,128)(2,1)S(1)}) custom-call(bf16[16,288,128]{2,1,0:T(8,128)(2,1)} %all-to-all-done.kt_ref, bf16[8,288,512]{2,1,0:T(8,128)(2,1)S(1)} %queries.1.q0_ref.qb_ref.qa_ref, bf16[8,288,512]{2,1,0:T(8,128)(2,1)S(1)} %queries.1.q0_ref.qb_ref.qa_ref, ...), custom_call_target="tpu_custom_call" | custom-call | tf_op jit(solution)/shard_map/attend/pallas_call | solution.py:345
  51.9 0.0 copy-start
  51.9 38.0 %all_to_all.15.rows_ref = bf16[128,8,1024]{2,1,0:T(8,128)(2,1)S(1)} all-to-all(bf16[128,8,1024]{2,1,0:T(8,128)(2,1)S(1)} %bitcast.27), channel_id=1, replica_groups=mesh['sp'=16,'dp'=8] {'sp','dp'}, dimensions={0} | all-to-all | bytes 4194304 | tf_op jit(solution)/shard_map/all_to_all | solution.py:412
  89.9 0.0 copy-done.1
  89.9 0.0 copy-done
  89.9 9.0 %experts.1 = bf16[128,8,1024]{2,1,0:T(8,128)(2,1)S(1)} custom-call(bf16[128,8,1024]{2,1,0:T(8,128)(2,1)S(1)} %all_to_all.15.rows_ref, bf16[2048,1024]{1,0:T(8,128)(2,1)S(1)} %bitcast.25, bf16[2048,1024]{1,0:T(8,128)(2,1)S(1)} %bitcast.26, bf16[1024,2048]{1,0:T(8,128)(2,1)} %bitcast.30), custom_call_target="tpu_custom_call" | custom-call | tf_op jit(solution)/shard_map/experts/pallas_call | solution.py:418
  99.0 0.0 copy-start.4
  99.0 0.0 copy-start.5
  99.0 34.5 %all_to_all.16 = bf16[128,8,1024]{2,1,0:T(8,128)(2,1)S(1)} all-to-all(bf16[128,8,1024]{2,1,0:T(8,128)(2,1)S(1)} %experts.1), channel_id=1, replica_groups=mesh['sp'=16,'dp'=8] {'sp','dp'}, dimensions={0} | all-to-all | bytes 4194304 | tf_op jit(solution)/shard_map/all_to_all | solution.py:439
  133.5 0.0 copy-done.4
  133.5 0.0 copy-done.5
  133.5 3.1 %combine.1 = bf16[128,2048]{1,0:T(8,128)(2,1)} custom-call(bf16[1024,1024]{1,0:T(8,128)(2,1)S(1)} %bitcast.24, s32[128,2]{1,0:T(8,128)S(1)} %copy-done.4, f32[128,2]{1,0:T(8,128)S(1)} %copy-done.5, f32[128,2048]{1,0:T(8,128)S(1)} %get-tuple-element.19.mixed_ref), custom_call_target="tpu_custom_call" | custom-call | tf_op jit(solution)/shard_map/combine/pallas_call | solution.py:441
Async XLA Ops:
  0.6 11.1 %copy-start.12 = (f32[1,128,2]{1,2,0:T(2,128)S(1)}, f32[1,128,2]{1,2,0:T(2,128)}, u32[]{:S(2)}) copy-start(f32[1,128,2]{1,2,0:T(2,128)} %param.25) | copy-start | bytes 3076
  0.6 11.8 %copy-start.11 = (s32[1,128,2]{1,2,0:T(2,128)S(1)}, s32[1,128,2]{1,2,0:T(2,128)}, u32[]{:S(2)}) copy-start(s32[1,128,2]{1,2,0:T(2,128)} %param.24) | copy-start | bytes 3076
  0.7 12.5 %copy-start.10 = (bf16[256,2048]{1,0:T(8,128)(2,1)S(1)}, bf16[256,2048]{1,0:T(8,128)(2,1)}, u32[]{:S(2)}) copy-start(bf16[256,2048]{1,0:T(8,128)(2,1)} %param.20) | copy-start | bytes 3145732
  2.9 12.5 %copy-start.6 = (f32[32,128]{1,0:T(8,128)S(1)}, f32[32,128]{1,0:T(8,128)}, u32[]{:S(2)}) copy-start(f32[32,128]{1,0:T(8,128)} %get-tuple-element.12.cos_ref) | copy-start | bytes 49156
  2.9 12.5 %copy-start.7 = (f32[32,128]{1,0:T(8,128)S(1)}, f32[32,128]{1,0:T(8,128)}, u32[]{:S(2)}) copy-start(f32[32,128]{1,0:T(8,128)} %get-tuple-element.13.sin_ref) | copy-start | bytes 49156
  2.9 26.3 %all-to-all-start = ((bf16[16,288,128]{2,1,0:T(8,128)(2,1)}), bf16[16,288,128]{2,1,0:T(8,128)(2,1)}, u32[]{:S(2)}, u32[]{:S(2)}) async-start(bf16[16,288,128]{2,1,0:T(8,128)(2,1)} %get-tuple-element.11), calls=%async_computation | async-start | bytes 2359296 | tf_op jit(solution)/shard_map/all_to_all | solution.py:397
  15.4 1.2 copy-start.2
  16.6 1.1 copy-start.3
  17.8 11.4 %copy-start.8 = (f32[2048]{0:T(1024)S(1)}, f32[2048]{0:T(1024)}, u32[]{:S(2)}) copy-start(f32[2048]{0:T(1024)} %param.23) | copy-start | bytes 24580
  17.8 11.4 %copy-start.9 = (s32[2,128]{1,0:T(2,128)S(1)}, s32[2,128]{1,0:T(2,128)}, u32[]{:S(2)}) copy-start(s32[2,128]{1,0:T(2,128)} %get-tuple-element.14.brow_ref) | copy-start | bytes 3076
  29.2 60.7 %copy-start.1 = (bf16[1,2048,1024]{2,1,0:T(8,128)(2,1)S(1)}, bf16[1,2048,1024]{2,1,0:T(8,128)(2,1)}, u32[]{:S(2)}) copy-start(bf16[1,2048,1024]{2,1,0:T(8,128)(2,1)} %param.27) | copy-start | bytes 12582916
  51.9 38.0 %copy-start = (bf16[1,2048,1024]{2,1,0:T(8,128)(2,1)S(1)}, bf16[1,2048,1024]{2,1,0:T(8,128)(2,1)}, u32[]{:S(2)}) copy-start(bf16[1,2048,1024]{2,1,0:T(8,128)(2,1)} %param.26) | copy-start | bytes 12582916
  99.0 34.5 %copy-start.4 = (s32[128,2]{1,0:T(8,128)S(1)}, s32[128,2]{1,0:T(8,128)}, u32[]{:S(2)}) copy-start(s32[128,2]{1,0:T(8,128)} %get-tuple-element.17.bcol_ref) | copy-start | bytes 3076
  99.0 34.5 %copy-start.5 = (f32[128,2]{1,0:T(8,128)S(1)}, f32[128,2]{1,0:T(8,128)}, u32[]{:S(2)}) copy-start(f32[128,2]{1,0:T(8,128)} %get-tuple-element.18.weight_ref) | copy-start | bytes 3076

commit v4 on v3

--- a/solution.py
+++ b/solution.py
@@ -18,6 +18,9 @@
 CAP = 4
 GROUP = 4
 CHUNK = 256
+F_STEPS = 1
+O_STEPS = 2
+PER = 1
 EPS = 1e-06
 CLAMP = 7.0
 ALPHA = 1.702
@@ -107,11 +110,15 @@
 
 
 def attend_kernel(
-    kt_ref, q0_ref, qb_ref, qa_ref, vb_ref, va_ref, vl_ref, wb_ref, wa_ref, wl_ref, res_ref,
-    gain_ref, brow_ref, mixed_ref, normed_ref, out_ref,
-    keys_ref, klt_ref, sa_ref, sb_ref, pa_ref, pb_ref, ta_ref, lb_ref, acc_ref,
+    kt_ref, q_ref, vb_ref, va_ref, vl_ref, w_hbm, res_ref, gain_ref, brow_ref, mixed_ref, normed_ref, out_ref,
+    keys_ref, klt_ref, sa_ref, sb_ref, pa_ref, pb_ref, ta_ref, lb_ref, acc_ref, w_ref, sem_ref,
 ):
     g = pl.program_id(0)
+    parts = (pl.ds(0, GROUP * PLAIN), pl.ds(GROUP * PLAIN, D - GROUP * PLAIN))
+    w_first, w_rest = [
+        pltpu.make_async_copy(w_hbm.at[part], w_ref.at[part], sem_ref.at[i])
+        for i, part in enumerate(parts)
+    ]
     last = pl.num_programs(0) - 1
     toks = res_ref.shape[0]
     n_keys = keys_ref.shape[0]
@@ -139,65 +146,71 @@
         ctx = dot(klt_ref[...], p_ref[...], ((1,), (0,)))
         return (ctx * (1.0 / jnp.sum(total, axis=0, keepdims=True))).astype(BF)
 
-    def heads_of(ctx, vt):
-        full_out = dot(vt, ctx, ((1,), (0,)))
+    def rows_of(group):
+        return pl.ds(pl.multiple_of(group * GROUP * PLAIN, GROUP * PLAIN), GROUP * PLAIN)
+
+    def heads_of(ctx, v_ref):
+        full_out = dot(v_ref[...], ctx, ((1,), (0,)))
         own = [
             full_out[j * PLAIN : (j + 1) * PLAIN, j * toks : (j + 1) * toks] for j in range(GROUP)
         ]
         return jnp.concatenate(own, axis=0).astype(BF)
 
-    def project(heads, w_ref):
-        acc_ref[...] += dot(heads, w_ref[...], ((0,), (0,)))
-
-    def stage(q_ref, s_new, s_old, p_new, p_old, top_old, total_old, v_ref, w_ref):
+    def project(heads, group):
+        acc_ref[...] += dot(heads, w_ref[rows_of(group), :], ((0,), (0,)))
+
+    def stage(after, s_new, s_old, p_new, p_old, top_old, total_old, v_ref, group):
         top, total, ctx, heads = None, None, None, None
         for i in range(chunks):
-            if q_ref is not None:
-                top = score_chunk(q_ref[0], s_new, i, top)
+            if after is not None:
+                top = score_chunk(q_ref[after], s_new, i, top)
             total = prob_chunk(s_old, p_new, i, top_old, total)
             if i == chunks // 8:
                 ctx = context(p_old, total_old)
             if i == chunks // 2:
-                heads = heads_of(ctx, v_ref[...])
+                heads = heads_of(ctx, v_ref)
             if i == chunks * 3 // 4:
-                project(heads, w_ref)
-        if q_ref is not None:
+                project(heads, group)
+        if after is not None:
             top = jnp.max(top, axis=0, keepdims=True)
         return top, total
 
     @pl.when(g == 0)
     def _():
+        w_first.start()
+        w_rest.start()
         for i in range(kt_ref.shape[0]):
             rows = slice(i * toks, (i + 1) * toks)
             klt_ref[:, rows] = kt_ref[i, :LAT, :]
             keys_ref[rows, :] = kt_ref[i].T
         top = None
         for i in range(chunks):
-            top = score_chunk(q0_ref[0], sa_ref, i, top)
+            top = score_chunk(q_ref[0], sa_ref, i, top)
         ta_ref[...] = jnp.max(top, axis=0, keepdims=True)
+        w_first.wait()
 
     top_b, total_a = stage(
-        qb_ref, sb_ref, sa_ref, pa_ref, pb_ref, ta_ref[...], lb_ref[...], vb_ref, wb_ref
+        2 * g + 1, sb_ref, sa_ref, pa_ref, pb_ref, ta_ref[...], lb_ref[...], vb_ref,
+        jnp.maximum(2 * g - 1, 0),
     )
 
     @pl.when(g == 0)
     def _():
+        w_rest.wait()
         acc_ref[...] = res_ref[...].astype(F32)
 
     @pl.when(g < last)
     def _():
         top_a, total_b = stage(
-            qa_ref, sa_ref, sb_ref, pb_ref, pa_ref, top_b, total_a, va_ref, wa_ref
+            2 * g + 2, sa_ref, sb_ref, pb_ref, pa_ref, top_b, total_a, va_ref, 2 * g
         )
         ta_ref[...] = top_a
         lb_ref[...] = total_b
 
     @pl.when(g == last)
     def _():
-        _, total_b = stage(
-            None, sa_ref, sb_ref, pb_ref, pa_ref, top_b, total_a, va_ref, wa_ref
-        )
-        project(heads_of(context(pb_ref, total_b), vl_ref[...]), wl_ref)
+        _, total_b = stage(None, sa_ref, sb_ref, pb_ref, pa_ref, top_b, total_a, va_ref, 2 * g)
+        project(heads_of(context(pb_ref, total_b), vl_ref), 2 * g + 1)
         mixed = acc_ref[...]
         mixed_ref[...] = mixed
         ms = jnp.mean(mixed * mixed, axis=-1, keepdims=True)
@@ -338,24 +351,17 @@
     toks = res.shape[0]
     keys_n = keys.shape[0] * toks
     groups = HEADS // GROUP
-    before = lambda g: jnp.maximum(2 * g - 1, 0)
-    q_at = lambda f: pl.BlockSpec((1, LAT + ROT, GROUP * toks), lambda g: (f(g), 0, 0))
     v_at = lambda f: pl.BlockSpec((GROUP * PLAIN, LAT), lambda g: (f(g), 0))
-    w_at = lambda f: pl.BlockSpec((GROUP * PLAIN, D), lambda g: (f(g), 0))
     return pl.pallas_call(
         attend_kernel,
         grid=(groups // 2,),
         in_specs=[
             whole(),
-            q_at(lambda g: 0),
-            q_at(lambda g: 2 * g + 1),
-            q_at(lambda g: jnp.minimum(2 * g + 2, groups - 1)),
-            v_at(before),
+            whole(),
+            v_at(lambda g: jnp.maximum(2 * g - 1, 0)),
             v_at(lambda g: 2 * g),
             v_at(lambda g: groups - 1),
-            w_at(before),
-            w_at(lambda g: 2 * g),
-            w_at(lambda g: groups - 1),
+            pl.BlockSpec(memory_space=pl.ANY),
             full(toks, D),
             full(1, D),
             full(TOPK, toks),
@@ -372,10 +378,60 @@
             pltpu.VMEM((1, GROUP * toks), F32),
             pltpu.VMEM((8, GROUP * toks), F32),
             pltpu.VMEM((toks, D), F32),
+            pltpu.VMEM((D, D), BF),
+            pltpu.SemaphoreType.DMA((2,)),
         ],
         compiler_params=params(44),
         name="attend",
-    )(keys, qs, qs, qs, vut, vut, vut, wo, wo, wo, res, gain, brow)
+    )(keys, in_vmem(qs), vut, vut, vut, in_hbm(wo), res, in_hbm(gain), in_hbm(brow))
+
+
+def run_experts(slot_rows, gate, up, down, f_steps, o_steps):
+    sds = jax.ShapeDtypeStruct
+    experts = slot_rows.shape[0]
+    fb, lanes = FF // f_steps, D // 2 // o_steps
+    out_at = lambda f: jnp.maximum(f - f_steps, 0)
+    return pl.pallas_call(
+        expert_kernel,
+        grid=(f_steps + o_steps,),
+        in_specs=[whole()] * 2 + [pl.BlockSpec(memory_space=pl.ANY)] * 2,
+        out_specs=pl.BlockSpec((experts, 8, lanes), lambda f: (0, 0, out_at(f))),
+        out_shape=sds((experts, 8, D // 2), BF),
+        scratch_shapes=[
+            pltpu.VMEM((experts * CAP, D), BF),
+            pltpu.VMEM((f_steps, experts * CAP, fb), BF),
+            pltpu.VMEM((D, FF), BF),
+            pltpu.VMEM((FF, D), BF),
+            pltpu.SemaphoreType.DMA((2,)),
+        ],
+        compiler_params=params(40),
+        name="experts",
+    )(
+        in_vmem(slot_rows),
+        in_vmem(gate),
+        up,
+        down,
+    )
+
+
+def run_combine(rows, bcol, wcol, mixed, per):
+    toks = mixed.shape[0]
+    n_rows = rows.shape[0]
+    return pl.pallas_call(
+        combine_kernel,
+        grid=(2 * per,),
+        in_specs=[
+            whole(),
+            full(toks, TOPK),
+            full(toks, TOPK),
+            pl.BlockSpec((toks, D // 2 // per), lambda n: (0, n)),
+        ],
+        out_specs=pl.BlockSpec((toks, D // 2 // per), lambda n: (0, n)),
+        out_shape=jax.ShapeDtypeStruct((toks, D), BF),
+        scratch_shapes=[pltpu.VMEM((TOPK * toks, n_rows), BF)],
+        compiler_params=params(40),
+        name="combine",
+    )(in_vmem(rows), bcol, wcol, mixed)
 
 
 def local(
@@ -412,47 +468,11 @@
     slot_rows = lax.all_to_all(
         outgoing.reshape(experts, 8, D // 2), ("sp", "dp"), 0, 0, tiled=True
     )
-    f_steps, o_steps = 4, 2
-    fb, lanes = FF // f_steps, D // 2 // o_steps
-    out_at = lambda f: jnp.maximum(f - f_steps, 0)
-    expert_out = pl.pallas_call(
-        expert_kernel,
-        grid=(f_steps + o_steps,),
-        in_specs=[whole()] * 2 + [pl.BlockSpec(memory_space=pl.ANY)] * 2,
-        out_specs=pl.BlockSpec((experts, 8, lanes), lambda f: (0, 0, out_at(f))),
-        out_shape=sds((experts, 8, D // 2), BF),
-        scratch_shapes=[
-            pltpu.VMEM((experts * CAP, D), BF),
-            pltpu.VMEM((f_steps, experts * CAP, fb), BF),
-            pltpu.VMEM((D, FF), BF),
-            pltpu.VMEM((FF, D), BF),
-            pltpu.SemaphoreType.DMA((2,)),
-        ],
-        compiler_params=params(40),
-        name="experts",
-    )(
-        in_vmem(slot_rows),
-        in_vmem(expert_gate[0]),
-        expert_up[0],
-        expert_down[0],
+    expert_out = run_experts(
+        slot_rows, expert_gate[0], expert_up[0], expert_down[0], F_STEPS, O_STEPS
     )
     returned = lax.all_to_all(expert_out, ("sp", "dp"), 0, 0, tiled=True)
-    per = 2
-    layer_out = pl.pallas_call(
-        combine_kernel,
-        grid=(2 * per,),
-        in_specs=[
-            whole(),
-            full(toks, TOPK),
-            full(toks, TOPK),
-            pl.BlockSpec((toks, D // 2 // per), lambda n: (0, n)),
-        ],
-        out_specs=pl.BlockSpec((toks, D // 2 // per), lambda n: (0, n)),
-        out_shape=sds((toks, D), BF),
-        scratch_shapes=[pltpu.VMEM((TOPK * toks, experts * 8), BF)],
-        compiler_params=params(40),
-        name="combine",
-    )(in_vmem(returned.reshape(experts * 8, D // 2)), bcol, wcol, mixed)
+    layer_out = run_combine(returned.reshape(experts * 8, D // 2), bcol, wcol, mixed, PER)
     return normed[None], layer_out[None]
 
 

time: 137 us -> 135 us (0.985)
  Pallas kernels: 41.8 us -> 39.6 us
    pallas_call x3, Pallas kernels: 34.8 us -> 32.6 us  [the longest x1 21.9 us: attend(): pl.pallas_call(attend_kernel, grid=(groups // 2,), in_specs=[whole(), who...]
    unnamed x28 -> x24, local copies, waits for them, and re-layouts: 3.66 us -> 3.65 us
  transfers between devices with their start and end apart: 1 -> 1, of which waited for: 1 -> 1; matrix products, arithmetic and copies ran while one was open for 1% -> 1% of each run, Pallas kernels for 3% -> 4%
where the time goes in v4:
time: 135 us; the launch traced here: 134 us
  blocking collectives  72.5 us (54%)
  Pallas kernels  39.6 us (29%)
  starting transfers between devices  8.76 us (6%)
  waiting for transfers between devices  8.38 us (6%)
  local copies, waits for them, and re-layouts  4.39 us (3%)
    all_to_all x1, blocking collectives, local(): lax.all_to_all(outgoing.reshape(experts, 8, D // 2), ('sp', 'dp'), 0, 0,...  38 us
    all_to_all x1, blocking collectives, local(): returned = lax.all_to_all(expert_out, ('sp', 'dp'), 0, 0, tiled=True)  34.5 us
    pallas_call x1, Pallas kernels, attend(): pl.pallas_call(attend_kernel, grid=(groups // 2,), in_specs=[whole(), who...  21.9 us
    all_to_all x1, starting transfers between devices, local(): keys = in_vmem(lax.all_to_all(packed, 'sp', 0, 0, tiled=True))  8.76 us
    all_to_all x1, waiting for transfers between devices, local(): keys = in_vmem(lax.all_to_all(packed, 'sp', 0, 0, tiled=True))  8.38 us
    pallas_call x1, Pallas kernels, run_experts(): pl.pallas_call(expert_kernel, grid=(f_steps + o_steps,), in_specs=[whole(...  8.37 us
    unnamed x24, local copies, waits for them, and re-layouts  3.65 us
    pallas_call x1, Pallas kernels, ready_queries(): pl.pallas_call(query_kernel, grid=(HEADS // GROUP,), in_specs=[pl.BlockSp...  3.02 us
  transfers between devices with their start and end apart: 1, of which 1 were waited for; matrix products, arithmetic and copies ran while one was open for 1% of the time, Pallas kernels for 4%

profile of v4, /device:TPU:1, one launch (start us, length us, event | category | flops | bytes accessed | tf_op | source)
XLA Modules:
  0.0 134.4 jit_solution(8233498503903712236)
XLA Ops:
  0.6 0.0 copy-start.10
  0.6 0.0 copy-start.9
  0.7 0.0 copy-start.8
  0.7 2.2 %prep.1 = (bf16[16,288,128]{2,1,0:T(8,128)(2,1)}, f32[32,128]{1,0:T(8,128)}, f32[32,128]{1,0:T(8,128)}) custom-call(s32[1]{0:T(128)} %bitcast.off_ref, bf16[128,256]{1,0:T(8,128)(2,1)} %bitcast.33, bf16[32,128]{1,0:T(8,128)(2,1)} %bitcast.35, f32[1,256]{1,0:T(1,128)} %bitcast.38, f32[32,1]{1,0:T(8,128)} %constant.8.clone.freq_ref), custom_call_target="tpu_custom_call" | custom-call | tf_op jit(solution)/shard_map/prep/pallas_call | solution.py:446
  2.9 0.0 copy-start.6
  2.9 0.0 copy-start.7
  2.9 8.8 %all-to-all-start = ((bf16[16,288,128]{2,1,0:T(8,128)(2,1)}), bf16[16,288,128]{2,1,0:T(8,128)(2,1)}, u32[]{:S(2)}, u32[]{:S(2)}) async-start(bf16[16,288,128]{2,1,0:T(8,128)(2,1)} %get-tuple-element.11), calls=%async_computation | async-start | bytes 2359296 | tf_op jit(solution)/shard_map/all_to_all | solution.py:453
  11.7 0.0 copy-done.10
  11.7 0.7 copy.18
  12.4 0.0 copy-done.9
  12.4 0.7 copy.19.col_ref
  13.2 0.0 copy-done.8
  13.2 0.5 copy.17
  13.7 1.7 %routes.1 = (s32[128,2]{1,0:T(8,128)}, s32[2,128]{1,0:T(2,128)}, f32[128,2]{1,0:T(8,128)}) custom-call(s32[128,2]{1,0:T(8,128)} %copy.19.col_ref, s32[2,128]{1,0:T(2,128)} %bitcast.36, f32[128,2]{1,0:T(8,128)} %bitcast.32), custom_call_target="tpu_custom_call" | custom-call | tf_op jit(solution)/shard_map/routes/pallas_call | solution.py:454
  15.4 0.0 copy-done.6
  15.4 0.0 copy-done.7
  15.4 0.0 copy-start.2
  15.4 1.2 copy-done.2
  16.6 0.0 copy-start.3
  16.7 1.1 copy-done.3
  17.8 3.0 %queries.1.q_ref = bf16[8,288,512]{2,1,0:T(8,128)(2,1)S(1)} custom-call(bf16[128,3072]{1,0:T(8,128)(2,1)S(1)} %bitcast.28, f32[32,128]{1,0:T(8,128)S(1)} %copy-done.6, f32[32,128]{1,0:T(8,128)S(1)} %copy-done.7, bf16[256,2048]{1,0:T(8,128)(2,1)S(1)} %copy-done.2), custom_call_target="tpu_custom_call" | custom-call | tf_op jit(solution)/shard_map/queries/pallas_call | solution.py:332
  20.8 8.4 %all-to-all-done.kt_ref = bf16[16,288,128]{2,1,0:T(8,128)(2,1)} async-done(((bf16[16,288,128]{2,1,0:T(8,128)(2,1)}), bf16[16,288,128]{2,1,0:T(8,128)(2,1)}, u32[]{:S(2)}, u32[]{:S(2)}) %all-to-all-start) | async-done | bytes 1179680 | tf_op jit(solution)/shard_map/all_to_all | solution.py:453
  29.2 0.0 copy-start.1
  29.2 21.9 %attend.1 = (f32[128,2048]{1,0:T(8,128)S(1)}, bf16[128,2048]{1,0:T(8,128)(2,1)}, bf16[1024,1024]{1,0:T(8,128)(2,1)S(1)}) custom-call(bf16[16,288,128]{2,1,0:T(8,128)(2,1)} %all-to-all-done.kt_ref, bf16[8,288,512]{2,1,0:T(8,128)(2,1)S(1)} %queries.1.q_ref, bf16[2048,256]{1,0:T(8,128)(2,1)S(1)} %bitcast.21, bf16[2048,256]{1,0:T(8,128)(2,1)S(1)} %bitcast.22, ...), custom_call_target="tpu_custom_call" | custom-call | tf_op jit(solution)/shard_map/attend/pallas_call | solution.py:355
  51.1 0.0 copy-start
  51.1 38.0 %all_to_all.15.rows_ref = bf16[128,8,1024]{2,1,0:T(8,128)(2,1)S(1)} all-to-all(bf16[128,8,1024]{2,1,0:T(8,128)(2,1)S(1)} %bitcast.27), channel_id=1, replica_groups=mesh['sp'=16,'dp'=8] {'sp','dp'}, dimensions={0} | all-to-all | bytes 4194304 | tf_op jit(solution)/shard_map/all_to_all | solution.py:468
  89.1 0.0 copy-done.1
  89.1 0.0 copy-done
  89.1 8.4 %experts.1 = bf16[128,8,1024]{2,1,0:T(8,128)(2,1)S(1)} custom-call(bf16[128,8,1024]{2,1,0:T(8,128)(2,1)S(1)} %all_to_all.15.rows_ref, bf16[2048,1024]{1,0:T(8,128)(2,1)S(1)} %bitcast.25, bf16[2048,1024]{1,0:T(8,128)(2,1)S(1)} %bitcast.26, bf16[1024,2048]{1,0:T(8,128)(2,1)} %bitcast.29), custom_call_target="tpu_custom_call" | custom-call | tf_op jit(solution)/shard_map/experts/pallas_call | solution.py:394
  97.5 0.0 copy-start.4
  97.5 0.0 copy-start.5
  97.5 34.5 %all_to_all.16 = bf16[128,8,1024]{2,1,0:T(8,128)(2,1)S(1)} all-to-all(bf16[128,8,1024]{2,1,0:T(8,128)(2,1)S(1)} %experts.1), channel_id=1, replica_groups=mesh['sp'=16,'dp'=8] {'sp','dp'}, dimensions={0} | all-to-all | bytes 4194304 | tf_op jit(solution)/shard_map/all_to_all | solution.py:474
  132.0 0.0 copy-done.4
  132.0 0.0 copy-done.5
  132.0 2.4 %combine.1 = bf16[128,2048]{1,0:T(8,128)(2,1)} custom-call(bf16[1024,1024]{1,0:T(8,128)(2,1)S(1)} %bitcast.24, s32[128,2]{1,0:T(8,128)S(1)} %copy-done.4, f32[128,2]{1,0:T(8,128)S(1)} %copy-done.5, f32[128,2048]{1,0:T(8,128)S(1)} %get-tuple-element.19.mixed_ref), custom_call_target="tpu_custom_call" | custom-call | tf_op jit(solution)/shard_map/combine/pallas_call | solution.py:420
Async XLA Ops:
  0.6 11.1 %copy-start.10 = (f32[1,128,2]{1,2,0:T(2,128)S(1)}, f32[1,128,2]{1,2,0:T(2,128)}, u32[]{:S(2)}) copy-start(f32[1,128,2]{1,2,0:T(2,128)} %param.25) | copy-start | bytes 3076
  0.6 11.8 %copy-start.9 = (s32[1,128,2]{1,2,0:T(2,128)S(1)}, s32[1,128,2]{1,2,0:T(2,128)}, u32[]{:S(2)}) copy-start(s32[1,128,2]{1,2,0:T(2,128)} %param.24) | copy-start | bytes 3076
  0.7 12.5 %copy-start.8 = (bf16[256,2048]{1,0:T(8,128)(2,1)S(1)}, bf16[256,2048]{1,0:T(8,128)(2,1)}, u32[]{:S(2)}) copy-start(bf16[256,2048]{1,0:T(8,128)(2,1)} %param.20) | copy-start | bytes 3145732
  2.9 12.5 %copy-start.6 = (f32[32,128]{1,0:T(8,128)S(1)}, f32[32,128]{1,0:T(8,128)}, u32[]{:S(2)}) copy-start(f32[32,128]{1,0:T(8,128)} %get-tuple-element.12.cos_ref) | copy-start | bytes 49156
  2.9 12.5 %copy-start.7 = (f32[32,128]{1,0:T(8,128)S(1)}, f32[32,128]{1,0:T(8,128)}, u32[]{:S(2)}) copy-start(f32[32,128]{1,0:T(8,128)} %get-tuple-element.13.sin_ref) | copy-start | bytes 49156
  2.9 26.3 %all-to-all-start = ((bf16[16,288,128]{2,1,0:T(8,128)(2,1)}), bf16[16,288,128]{2,1,0:T(8,128)(2,1)}, u32[]{:S(2)}, u32[]{:S(2)}) async-start(bf16[16,288,128]{2,1,0:T(8,128)(2,1)} %get-tuple-element.11), calls=%async_computation | async-start | bytes 2359296 | tf_op jit(solution)/shard_map/all_to_all | solution.py:453
  15.4 1.2 copy-start.2
  16.6 1.1 copy-start.3
  29.2 59.9 %copy-start.1 = (bf16[1,2048,1024]{2,1,0:T(8,128)(2,1)S(1)}, bf16[1,2048,1024]{2,1,0:T(8,128)(2,1)}, u32[]{:S(2)}) copy-start(bf16[1,2048,1024]{2,1,0:T(8,128)(2,1)} %param.27) | copy-start | bytes 12582916
  51.1 38.0 %copy-start = (bf16[1,2048,1024]{2,1,0:T(8,128)(2,1)S(1)}, bf16[1,2048,1024]{2,1,0:T(8,128)(2,1)}, u32[]{:S(2)}) copy-start(bf16[1,2048,1024]{2,1,0:T(8,128)(2,1)} %param.26) | copy-start | bytes 12582916
  97.5 34.5 %copy-start.4 = (s32[128,2]{1,0:T(8,128)S(1)}, s32[128,2]{1,0:T(8,128)}, u32[]{:S(2)}) copy-start(s32[128,2]{1,0:T(8,128)} %get-tuple-element.17.bcol_ref) | copy-start | bytes 3076
  97.5 34.5 %copy-start.5 = (f32[128,2]{1,0:T(8,128)S(1)}, f32[128,2]{1,0:T(8,128)}, u32[]{:S(2)}) copy-start(f32[128,2]{1,0:T(8,128)} %get-tuple-element.18.weight_ref) | copy-start | bytes 3076

commit v5 on v4

--- a/solution.py
+++ b/solution.py
@@ -229,11 +229,10 @@
 
 
 def expert_kernel(
-    rows_ref, gate_ref, up_hbm, down_hbm, out_ref, x_ref, hidden_ref, up_ref, down_ref, sem_ref
+    rows_ref, gate_ref, up_ref, down_hbm, out_ref, x_ref, hidden_ref, down_ref, sem_ref
 ):
     f = pl.program_id(0)
-    copy_up = pltpu.make_async_copy(up_hbm, up_ref, sem_ref.at[0])
-    copy_down = pltpu.make_async_copy(down_hbm, down_ref, sem_ref.at[1])
+    copy_down = pltpu.make_async_copy(down_hbm, down_ref, sem_ref.at[0])
     n_src = rows_ref.shape[0]
     half_d = D // 2
     f_steps, _, fb = hidden_ref.shape
@@ -241,7 +240,6 @@
 
     @pl.when(f == 0)
     def _():
-        copy_up.start()
         copy_down.start()
         r = rows_ref[...].astype(F32).reshape(n_src // 2, 2, 8, half_d)
         a, b = r[:, 0], r[:, 1]
@@ -250,10 +248,6 @@
         second = jnp.where(low, pltpu.roll(a, 4, 1), b)
         x_ref[:, :half_d] = first.reshape(n_src * 4, half_d).astype(BF)
         x_ref[:, half_d:] = second.reshape(n_src * 4, half_d).astype(BF)
-
-    @pl.when(f == 0)
-    def _():
-        copy_up.wait()
 
     @pl.when(f == f_steps)
     def _():
@@ -394,23 +388,22 @@
     return pl.pallas_call(
         expert_kernel,
         grid=(f_steps + o_steps,),
-        in_specs=[whole()] * 2 + [pl.BlockSpec(memory_space=pl.ANY)] * 2,
+        in_specs=[whole()] * 3 + [pl.BlockSpec(memory_space=pl.ANY)],
         out_specs=pl.BlockSpec((experts, 8, lanes), lambda f: (0, 0, out_at(f))),
         out_shape=sds((experts, 8, D // 2), BF),
         scratch_shapes=[
             pltpu.VMEM((experts * CAP, D), BF),
             pltpu.VMEM((f_steps, experts * CAP, fb), BF),
-            pltpu.VMEM((D, FF), BF),
             pltpu.VMEM((FF, D), BF),
-            pltpu.SemaphoreType.DMA((2,)),
+            pltpu.SemaphoreType.DMA((1,)),
         ],
         compiler_params=params(40),
         name="experts",
     )(
         in_vmem(slot_rows),
         in_vmem(gate),
-        up,
-        down,
+        in_vmem(up),
+        in_hbm(down),
     )
 
 

time: 135 us -> 135 us (level)
  no operation moved by 1% of the time
where the time goes in v5:
time: 135 us; the launch traced here: 134 us
  blocking collectives  72.5 us (54%)
  Pallas kernels  39.3 us (29%)
  starting transfers between devices  8.76 us (6%)
  waiting for transfers between devices  8.38 us (6%)
  local copies, waits for them, and re-layouts  4.39 us (3%)
    all_to_all x1, blocking collectives, local(): lax.all_to_all(outgoing.reshape(experts, 8, D // 2), ('sp', 'dp'), 0, 0,...  38 us
    all_to_all x1, blocking collectives, local(): returned = lax.all_to_all(expert_out, ('sp', 'dp'), 0, 0, tiled=True)  34.5 us
    pallas_call x1, Pallas kernels, attend(): pl.pallas_call(attend_kernel, grid=(groups // 2,), in_specs=[whole(), who...  21.9 us
    all_to_all x1, starting transfers between devices, local(): keys = in_vmem(lax.all_to_all(packed, 'sp', 0, 0, tiled=True))  8.76 us
    all_to_all x1, waiting for transfers between devices, local(): keys = in_vmem(lax.all_to_all(packed, 'sp', 0, 0, tiled=True))  8.38 us
    pallas_call x1, Pallas kernels, run_experts(): pl.pallas_call(expert_kernel, grid=(f_steps + o_steps,), in_specs=[whole(...  8.08 us
    unnamed x24, local copies, waits for them, and re-layouts  3.65 us
    pallas_call x1, Pallas kernels, ready_queries(): pl.pallas_call(query_kernel, grid=(HEADS // GROUP,), in_specs=[pl.BlockSp...  3.02 us
  transfers between devices with their start and end apart: 1, of which 1 were waited for; matrix products, arithmetic and copies ran while one was open for 1% of the time, Pallas kernels for 4%

profile of v5, /device:TPU:1, one launch (start us, length us, event | category | flops | bytes accessed | tf_op | source)
XLA Modules:
  0.0 134.1 jit_solution(7483527433016399266)
XLA Ops:
  0.6 0.0 copy-start.10
  0.6 0.0 copy-start.9
  0.7 0.0 copy-start.8
  0.7 2.2 %prep.1 = (bf16[16,288,128]{2,1,0:T(8,128)(2,1)}, f32[32,128]{1,0:T(8,128)}, f32[32,128]{1,0:T(8,128)}) custom-call(s32[1]{0:T(128)} %bitcast.off_ref, bf16[128,256]{1,0:T(8,128)(2,1)} %bitcast.33, bf16[32,128]{1,0:T(8,128)(2,1)} %bitcast.35, f32[1,256]{1,0:T(1,128)} %bitcast.38, f32[32,1]{1,0:T(8,128)} %constant.8.clone.freq_ref), custom_call_target="tpu_custom_call" | custom-call | tf_op jit(solution)/shard_map/prep/pallas_call | solution.py:439
  2.9 0.0 copy-start.6
  2.9 0.0 copy-start.7
  2.9 8.8 %all-to-all-start = ((bf16[16,288,128]{2,1,0:T(8,128)(2,1)}), bf16[16,288,128]{2,1,0:T(8,128)(2,1)}, u32[]{:S(2)}, u32[]{:S(2)}) async-start(bf16[16,288,128]{2,1,0:T(8,128)(2,1)} %get-tuple-element.11), calls=%async_computation | async-start | bytes 2359296 | tf_op jit(solution)/shard_map/all_to_all | solution.py:446
  11.7 0.0 copy-done.10
  11.7 0.7 copy.18
  12.4 0.0 copy-done.9
  12.4 0.7 copy.19.col_ref
  13.2 0.0 copy-done.8
  13.2 0.5 copy.17
  13.7 1.7 %routes.1 = (s32[128,2]{1,0:T(8,128)}, s32[2,128]{1,0:T(2,128)}, f32[128,2]{1,0:T(8,128)}) custom-call(s32[128,2]{1,0:T(8,128)} %copy.19.col_ref, s32[2,128]{1,0:T(2,128)} %bitcast.36, f32[128,2]{1,0:T(8,128)} %bitcast.32), custom_call_target="tpu_custom_call" | custom-call | tf_op jit(solution)/shard_map/routes/pallas_call | solution.py:447
  15.4 0.0 copy-done.6
  15.4 0.0 copy-done.7
  15.4 0.0 copy-start.2
  15.4 1.2 copy-done.2
  16.6 0.0 copy-start.3
  16.7 1.1 copy-done.3
  17.8 3.0 %queries.1.q_ref = bf16[8,288,512]{2,1,0:T(8,128)(2,1)S(1)} custom-call(bf16[128,3072]{1,0:T(8,128)(2,1)S(1)} %bitcast.28, f32[32,128]{1,0:T(8,128)S(1)} %copy-done.6, f32[32,128]{1,0:T(8,128)S(1)} %copy-done.7, bf16[256,2048]{1,0:T(8,128)(2,1)S(1)} %copy-done.2), custom_call_target="tpu_custom_call" | custom-call | tf_op jit(solution)/shard_map/queries/pallas_call | solution.py:326
  20.8 8.4 %all-to-all-done.kt_ref = bf16[16,288,128]{2,1,0:T(8,128)(2,1)} async-done(((bf16[16,288,128]{2,1,0:T(8,128)(2,1)}), bf16[16,288,128]{2,1,0:T(8,128)(2,1)}, u32[]{:S(2)}, u32[]{:S(2)}) %all-to-all-start) | async-done | bytes 1179680 | tf_op jit(solution)/shard_map/all_to_all | solution.py:446
  29.2 0.0 copy-start.1
  29.2 21.9 %attend.1 = (f32[128,2048]{1,0:T(8,128)S(1)}, bf16[128,2048]{1,0:T(8,128)(2,1)}, bf16[1024,1024]{1,0:T(8,128)(2,1)S(1)}) custom-call(bf16[16,288,128]{2,1,0:T(8,128)(2,1)} %all-to-all-done.kt_ref, bf16[8,288,512]{2,1,0:T(8,128)(2,1)S(1)} %queries.1.q_ref, bf16[2048,256]{1,0:T(8,128)(2,1)S(1)} %bitcast.21, bf16[2048,256]{1,0:T(8,128)(2,1)S(1)} %bitcast.22, ...), custom_call_target="tpu_custom_call" | custom-call | tf_op jit(solution)/shard_map/attend/pallas_call | solution.py:349
  51.1 0.0 copy-start
  51.1 38.0 %all_to_all.15.rows_ref = bf16[128,8,1024]{2,1,0:T(8,128)(2,1)S(1)} all-to-all(bf16[128,8,1024]{2,1,0:T(8,128)(2,1)S(1)} %bitcast.27), channel_id=1, replica_groups=mesh['sp'=16,'dp'=8] {'sp','dp'}, dimensions={0} | all-to-all | bytes 4194304 | tf_op jit(solution)/shard_map/all_to_all | solution.py:461
  89.1 0.0 copy-done.1
  89.1 0.0 copy-done
  89.1 8.1 %experts.1 = bf16[128,8,1024]{2,1,0:T(8,128)(2,1)S(1)} custom-call(bf16[128,8,1024]{2,1,0:T(8,128)(2,1)S(1)} %all_to_all.15.rows_ref, bf16[2048,1024]{1,0:T(8,128)(2,1)S(1)} %bitcast.25, bf16[2048,1024]{1,0:T(8,128)(2,1)S(1)} %bitcast.26, bf16[1024,2048]{1,0:T(8,128)(2,1)} %bitcast.29), custom_call_target="tpu_custom_call" | custom-call | tf_op jit(solution)/shard_map/experts/pallas_call | solution.py:388
  97.2 0.0 copy-start.4
  97.2 0.0 copy-start.5
  97.2 34.5 %all_to_all.16 = bf16[128,8,1024]{2,1,0:T(8,128)(2,1)S(1)} all-to-all(bf16[128,8,1024]{2,1,0:T(8,128)(2,1)S(1)} %experts.1), channel_id=1, replica_groups=mesh['sp'=16,'dp'=8] {'sp','dp'}, dimensions={0} | all-to-all | bytes 4194304 | tf_op jit(solution)/shard_map/all_to_all | solution.py:467
  131.7 0.0 copy-done.4
  131.7 0.0 copy-done.5
  131.7 2.4 %combine.1 = bf16[128,2048]{1,0:T(8,128)(2,1)} custom-call(bf16[1024,1024]{1,0:T(8,128)(2,1)S(1)} %bitcast.24, s32[128,2]{1,0:T(8,128)S(1)} %copy-done.4, f32[128,2]{1,0:T(8,128)S(1)} %copy-done.5, f32[128,2048]{1,0:T(8,128)S(1)} %get-tuple-element.19.mixed_ref), custom_call_target="tpu_custom_call" | custom-call | tf_op jit(solution)/shard_map/combine/pallas_call | solution.py:413
Async XLA Ops:
  0.6 11.1 %copy-start.10 = (f32[1,128,2]{1,2,0:T(2,128)S(1)}, f32[1,128,2]{1,2,0:T(2,128)}, u32[]{:S(2)}) copy-start(f32[1,128,2]{1,2,0:T(2,128)} %param.25) | copy-start | bytes 3076
  0.6 11.8 %copy-start.9 = (s32[1,128,2]{1,2,0:T(2,128)S(1)}, s32[1,128,2]{1,2,0:T(2,128)}, u32[]{:S(2)}) copy-start(s32[1,128,2]{1,2,0:T(2,128)} %param.24) | copy-start | bytes 3076
  0.7 12.5 %copy-start.8 = (bf16[256,2048]{1,0:T(8,128)(2,1)S(1)}, bf16[256,2048]{1,0:T(8,128)(2,1)}, u32[]{:S(2)}) copy-start(bf16[256,2048]{1,0:T(8,128)(2,1)} %param.20) | copy-start | bytes 3145732
  2.9 12.5 %copy-start.6 = (f32[32,128]{1,0:T(8,128)S(1)}, f32[32,128]{1,0:T(8,128)}, u32[]{:S(2)}) copy-start(f32[32,128]{1,0:T(8,128)} %get-tuple-element.12.cos_ref) | copy-start | bytes 49156
  2.9 12.5 %copy-start.7 = (f32[32,128]{1,0:T(8,128)S(1)}, f32[32,128]{1,0:T(8,128)}, u32[]{:S(2)}) copy-start(f32[32,128]{1,0:T(8,128)} %get-tuple-element.13.sin_ref) | copy-start | bytes 49156
  2.9 26.3 %all-to-all-start = ((bf16[16,288,128]{2,1,0:T(8,128)(2,1)}), bf16[16,288,128]{2,1,0:T(8,128)(2,1)}, u32[]{:S(2)}, u32[]{:S(2)}) async-start(bf16[16,288,128]{2,1,0:T(8,128)(2,1)} %get-tuple-element.11), calls=%async_computation | async-start | bytes 2359296 | tf_op jit(solution)/shard_map/all_to_all | solution.py:446
  15.4 1.2 copy-start.2
  16.6 1.1 copy-start.3
  29.2 59.9 %copy-start.1 = (bf16[1,2048,1024]{2,1,0:T(8,128)(2,1)S(1)}, bf16[1,2048,1024]{2,1,0:T(8,128)(2,1)}, u32[]{:S(2)}) copy-start(bf16[1,2048,1024]{2,1,0:T(8,128)(2,1)} %param.27) | copy-start | bytes 12582916
  51.1 38.0 %copy-start = (bf16[1,2048,1024]{2,1,0:T(8,128)(2,1)S(1)}, bf16[1,2048,1024]{2,1,0:T(8,128)(2,1)}, u32[]{:S(2)}) copy-start(bf16[1,2048,1024]{2,1,0:T(8,128)(2,1)} %param.26) | copy-start | bytes 12582916
  97.2 34.5 %copy-start.4 = (s32[128,2]{1,0:T(8,128)S(1)}, s32[128,2]{1,0:T(8,128)}, u32[]{:S(2)}) copy-start(s32[128,2]{1,0:T(8,128)} %get-tuple-element.17.bcol_ref) | copy-start | bytes 3076
  97.2 34.5 %copy-start.5 = (f32[128,2]{1,0:T(8,128)S(1)}, f32[128,2]{1,0:T(8,128)}, u32[]{:S(2)}) copy-start(f32[128,2]{1,0:T(8,128)} %get-tuple-element.18.weight_ref) | copy-start | bytes 3076
